TPU v7x, 32 devices: a whole 2x2x4 slice. The times are simulated.
32 devices in a mesh: sp: 8 (over z, x), tp: 4 (over y, core).
Axes of the slice: x: 2, y: 2, z: 4, core: 2. Of those that a mesh axis runs over, the one named last changes fastest.
Arguments:
- x_res: bfloat16 [2048, 2048], P(('sp', 'tp')), may hold values from -6 to 6
- q_a: bfloat16 [2048, 1024], P('sp', 'tp'), may hold values from -48 to 48
- k_a: bfloat16 [2048, 256], P('sp', 'tp'), may hold values from -48 to 48
- v_a: bfloat16 [2048, 256], P('sp', 'tp'), may hold values from -6 to 6
- q_b: bfloat16 [2048, 1024], P('sp', 'tp'), may hold values from -48 to 48
- k_b: bfloat16 [2048, 512], P('sp', 'tp'), may hold values from -48 to 48
- v_b: bfloat16 [2048, 512], P('sp', 'tp'), may hold values from -6 to 6
- gain_qa: float32 [64], replicated, may hold values from 1.2 to 6
- gain_ka: float32 [64], replicated, may hold values from 1.2 to 6
- gain_qb: float32 [128], replicated, may hold values from 1.2 to 6
- gain_kb: float32 [128], replicated, may hold values from 1.2 to 6
- w_out_a: bfloat16 [1024, 2048], P('tp'), may hold values from -0.125 to 0.125
- w_out_b: bfloat16 [1024, 2048], P('tp'), may hold values from -0.125 to 0.125
- gain_mid: float32 [2048], replicated, may hold values from 0.1 to 1.9
- w_gate: bfloat16 [2048, 3072], P('sp', 'tp'), may hold values from -0.125 to 0.125
- w_up: bfloat16 [2048, 3072], P('sp', 'tp'), may hold values from -0.125 to 0.125
- conv_gate: float32 [3, 3072], P(None, 'tp'), may hold values from -3.5 to 3.5
- conv_up: float32 [3, 3072], P(None, 'tp'), may hold values from -3.5 to 3.5
- w_down: bfloat16 [3072, 2048], P('tp', 'sp'), may hold values from -0.109375 to 0.109375
Outputs:
- layer_out: bfloat16 [2048, 2048], P(('sp', 'tp'))
All inputs are finite; a program needn't handle non-finite values.
Results may differ from a plain program's by a relative error of at most 0.014.
The roundings to bfloat16 on the way count: a program that leaves them out, or rounds other values in their place, can miss the bound.
Values may be sent and summed in bfloat16 or wider, within the bound.
A program may use at most 128 MiB of HBM per device.

v0:
```python
import functools

import jax
import jax.numpy as jnp
from jax import lax
from jax.experimental import pallas as pl
from jax.experimental.pallas import tpu as pltpu
from jax.sharding import PartitionSpec as P

DHA = 64
DHB = 128

norm_eps = 1e-06
rope_theta = 10000.0
F32 = jnp.float32
BF16 = jnp.bfloat16
MESH = pl.DeviceIdType.MESH
PIECES = 4


def rotary_angles(positions, head_size):
    half = head_size // 2
    inverse = jnp.power(jnp.float32(rope_theta), -jnp.arange(0, half, 2, dtype=jnp.float32) / half)
    grid_row = (positions // 64).astype(jnp.float32)[:, None] * inverse[None, :]
    grid_col = (positions % 64).astype(jnp.float32)[:, None] * inverse[None, :]
    return jnp.concatenate([grid_row, grid_row, grid_col, grid_col], axis=-1)


def lane_frequencies(head_size, width):
    half = head_size // 2
    inverse = jnp.power(jnp.float32(rope_theta), -jnp.arange(0, half, 2, dtype=jnp.float32) / half)
    return jnp.tile(inverse, width // inverse.shape[0])[None]


def block_mean(width, head):
    i = lax.broadcasted_iota(jnp.int32, (width, width), 0)
    j = lax.broadcasted_iota(jnp.int32, (width, width), 1)
    return jnp.where(lax.div(i, head) == lax.div(j, head), F32(1.0 / head), F32(0.0))


def block_turn(width, head):
    quarter = head // 4
    i = lax.broadcasted_iota(jnp.int32, (width, width), 0)
    j = lax.broadcasted_iota(jnp.int32, (width, width), 1)
    first = lax.rem(j, 2 * quarter) < quarter
    return jnp.where(
        first & (i == j + quarter),
        F32(-1.0),
        jnp.where(jnp.logical_not(first) & (i == j - quarter), F32(1.0), F32(0.0)),
    )


def exact_dot(a, b):
    return jnp.dot(a, b, precision=lax.Precision.HIGHEST, preferred_element_type=F32)


def prepared(raw, gain, angle_cos, angle_sin, head):
    width = raw.shape[1]
    values = raw.astype(F32)
    values = values * lax.rsqrt(exact_dot(values * values, block_mean(width, head)) + norm_eps)
    values = values * gain
    turned = exact_dot(values, block_turn(width, head))
    return (values * angle_cos + turned * angle_sin).astype(BF16)


def kernel(
    n, tp_n,
    x_ref, qa_ref, ka_hbm, va_hbm, qb_ref, kb_ref, vb_ref,
    gqa_ref, gka_ref, gqb_ref, gkb_ref,
    fra_ref, frb_ref,
    woa_hbm, wob_hbm, gmid_ref, wg_hbm, wu_hbm, cg_ref, cu_ref, wd_hbm,
    out_ref,
    ka_ref, va_ref, kv, qas, qbs, m_a, l_a, acc_a, m_b, l_b, acc_b,
    woa, wob, wg, wu, wdr, wdl,
    attn, part, rs_in, mid, nrm, acc_g, acc_u, joined, halo_lo, halo_hi, hidden, acc_d, part2, rs2_in,
    loc_sem, kv_send, kv_recv, w_send, w_recv, d_send, d_recv,
    rs_send, rs_recv, ag_send, ag_recv, h_send, h_recv, r2_send, r2_recv,
):
    sp = lax.axis_index("sp")
    tp = lax.axis_index("tp")
    rows = qa_ref.shape[0]
    own = x_ref.shape[0]
    half = n // 2

    odd = lax.rem(sp, 2)
    pos = (1 - odd) * lax.div(sp, 2) + odd * (n - 1 - lax.div(sp, 2))

    def at(p):
        p = lax.rem(p + 2 * n, n)
        back = lax.div(p, half)
        return (1 - back) * 2 * p + back * (2 * (n - 1 - p) + 1)

    right, left = at(pos + 1), at(pos - 1)
    above, below = lax.rem(sp + 1, n), lax.rem(sp + n - 1, n)

    barrier = pltpu.get_barrier_semaphore()
    for other in (right, left, above, below):
        pl.semaphore_signal(barrier, inc=1, device_id={"sp": other}, device_id_type=MESH)
    for d in range(1, tp_n):
        pl.semaphore_signal(
            barrier, inc=1, device_id={"tp": lax.rem(tp + d, tp_n)}, device_id_type=MESH
        )

    locals_ = [
        pltpu.make_async_copy(woa_hbm, woa, loc_sem.at[0]),
        pltpu.make_async_copy(wob_hbm, wob, loc_sem.at[1]),
        pltpu.make_async_copy(wg_hbm, wg.at[0], loc_sem.at[2]),
        pltpu.make_async_copy(wu_hbm, wu.at[0], loc_sem.at[3]),
        pltpu.make_async_copy(wd_hbm.at[pl.ds(0, wdr.shape[1])], wdr.at[0], loc_sem.at[4]),
        pltpu.make_async_copy(
            wd_hbm.at[pl.ds(wdr.shape[1], wdr.shape[1])], wdl.at[0], loc_sem.at[5]
        ),
    ]
    small = [
        pltpu.make_async_copy(ka_hbm, ka_ref, loc_sem.at[6]),
        pltpu.make_async_copy(va_hbm, va_ref, loc_sem.at[7]),
    ]
    for copy in locals_[2:4] + small + locals_[4:] + locals_[:2]:
        copy.start()

    def remote(src, dst, send, recv, **where):
        return pltpu.make_async_remote_copy(
            src_ref=src, dst_ref=dst, send_sem=send, recv_sem=recv,
            device_id=where, device_id_type=MESH,
        )

    def kv_r(s):
        return remote(kv.at[s - 1], kv.at[s], kv_send.at[s], kv_recv.at[s], sp=right)

    def kv_l(s):
        source = lax.rem(n - s + 1, n)
        return remote(kv.at[source], kv.at[n - s], kv_send.at[n - s], kv_recv.at[n - s], sp=left)

    wrows = wg.shape[1] // PIECES
    drows = wdr.shape[1] // PIECES

    def w_copy(s, p, direction):
        buf, to = (wg, right) if direction == 0 else (wu, left)
        cut = pl.ds(p * wrows, wrows)
        return remote(
            buf.at[s - 1, cut], buf.at[s, cut],
            w_send.at[direction, p, s], w_recv.at[direction, p, s], sp=to,
        )

    def d_copy(s, p, direction):
        buf, to = (wdr, right) if direction == 0 else (wdl, left)
        cut = pl.ds(p * drows, drows)
        return remote(
            buf.at[s - 1, cut], buf.at[s, cut],
            d_send.at[direction, p, s], d_recv.at[direction, p, s], sp=to,
        )

    def tick(copy, s, following=None):
        for p in range(PIECES):
            for direction in range(2):
                copy(s, p, direction).wait_recv()
                if following is None:
                    copy(s + 1, p, direction).start()
                elif following != "end":
                    following(1, p, direction).wait_recv()
                    following(2, p, direction).start()

    def begin(copy, s, low, high):
        for p in range(low, high):
            for direction in range(2):
                copy(s, p, direction).start()

    def pass_on(copy, s, low, high):
        for p in range(low, high):
            for direction in range(2):
                copy(s, p, direction).wait_recv()
                copy(s + 1, p, direction).start()

    pl.semaphore_wait(barrier, 4 + tp_n - 1)
    for copy in locals_[2:4]:
        copy.wait()
    begin(w_copy, 1, 0, PIECES // 2)

    def tables(freq_ref, head):
        shape = (rows, freq_ref.shape[1])
        token = lax.broadcasted_iota(jnp.int32, shape, 0) + sp * rows
        lane = lax.broadcasted_iota(jnp.int32, shape, 1)
        grid = jnp.where(lax.rem(lane, head) < head // 2, lax.div(token, 64), lax.rem(token, 64))
        angles = grid.astype(F32) * freq_ref[...]
        return jnp.cos(angles), jnp.sin(angles)

    ca, sa = tables(fra_ref, DHA)
    cb, sb = tables(frb_ref, DHB)
    for copy in small:
        copy.wait()
    wka, wkb = ka_ref.shape[1], kb_ref.shape[1]

    def wide(table, width):
        if width <= table.shape[1]:
            return table[:, :width]
        return jnp.concatenate([table] * (width // table.shape[1]), axis=1)

    def gains(ref, width):
        g = ref[...]
        count = width // g.shape[1]
        return g if count == 1 else jnp.concatenate([g] * count, axis=1)

    keys_a = prepared(ka_ref[...], gains(gka_ref, wka), wide(ca, wka), wide(sa, wka), DHA)
    keys_b = prepared(kb_ref[...], gains(gkb_ref, wkb), wide(cb, wkb), wide(sb, wkb), DHB)
    kv[0, :, :wkb] = keys_b
    kv[0, :, wkb:2 * wkb] = vb_ref[...]
    kv[0, :, 2 * wkb:] = jnp.concatenate([keys_a, va_ref[...]], axis=1)

    kv_r(1).start()
    kv_l(1).start()

    heads_a = qa_ref.shape[1] // DHA
    heads_b = qb_ref.shape[1] // DHB
    qa = prepared(
        qa_ref[...], gains(gqa_ref, heads_a * DHA), wide(ca, heads_a * DHA),
        wide(sa, heads_a * DHA), DHA,
    )
    qb = prepared(
        qb_ref[...], gains(gqb_ref, heads_b * DHB), wide(cb, heads_b * DHB),
        wide(sb, heads_b * DHB), DHB,
    )
    for h in range(heads_a):
        qas[h] = qa[:, h * DHA:(h + 1) * DHA]
    for h in range(heads_b):
        qbs[h] = qb[:, h * DHB:(h + 1) * DHB]
    for ref, low in ((m_a, -1e30), (m_b, -1e30), (l_a, 0.0), (l_b, 0.0), (acc_a, 0.0), (acc_b, 0.0)):
        ref[...] = jnp.full(ref.shape, low, F32)

    def attend_one(queries, key_rows, value_rows, m, l, acc, h):
        scale = F32(queries.shape[2] ** (-0.5))
        scores = lax.dot_general(
            queries[h], key_rows, (((1,), (1,)), ((), ())), preferred_element_type=F32
        ) * scale
        before = m[h]
        highest = jnp.maximum(before, jnp.max(scores, axis=-1, keepdims=True))
        factor = jnp.exp(before - highest)
        expd = jnp.exp(scores - highest)
        l[h] = l[h] * factor + jnp.sum(expd, axis=-1, keepdims=True)
        acc[h] = acc[h] * factor + jnp.dot(
            expd.astype(BF16), value_rows, preferred_element_type=F32
        )
        m[h] = highest

    def attend(slot):
        for h in range(heads_b):
            attend_one(qbs, kv[slot, :, :wkb], kv[slot, :, wkb:2 * wkb], m_b, l_b, acc_b, h)
        pair = kv[slot, :, 2 * wkb:]
        for h in range(heads_a):
            attend_one(qas, pair[:, :wka], pair[:, wka:], m_a, l_a, acc_a, h)

    attend(0)

    def kv_step(s, carry):
        kv_r(s).wait_recv()
        kv_r(s + 1).start()
        kv_l(s).wait_recv()

        @pl.when(s < half - 1)
        def _():
            kv_l(s + 1).start()

        @pl.when(s == 1)
        def _():
            begin(w_copy, 1, PIECES // 2, PIECES)

        @pl.when(s == 2)
        def _():
            begin(d_copy, 1, 0, PIECES)

        @pl.when(s == 3)
        def _():
            pass_on(w_copy, 1, 0, PIECES // 2)

        def one(i, inner):
            attend((1 - i) * s + i * (n - s))
            return inner

        lax.fori_loop(0, 2, one, 0)
        return carry

    for copy in locals_[:2] + locals_[4:]:
        copy.wait()
    lax.fori_loop(1, half, kv_step, 0)
    kv_r(half).wait_recv()
    pass_on(w_copy, 1, PIECES // 2, PIECES)
    attend(half)

    for h in range(heads_a):
        attn[:, h * DHA:(h + 1) * DHA] = (acc_a[h] / l_a[h]).astype(BF16)
    width_a = heads_a * DHA
    for h in range(heads_b):
        attn[:, width_a + h * DHB:width_a + (h + 1) * DHB] = (acc_b[h] / l_b[h]).astype(BF16)

    def rs_copy(d):
        to = lax.rem(tp + d, tp_n)
        return remote(
            part.at[pl.ds(pl.multiple_of(to * own, own), own)], rs_in.at[d - 1],
            rs_send.at[d - 1], rs_recv.at[d - 1], tp=to,
        )

    for i in range(tp_n):
        d = tp_n - 1 - i
        at_rows = pl.ds(pl.multiple_of(lax.rem(tp + d, tp_n) * own, own), own)
        block = attn[at_rows, :]
        part[at_rows, :] = (
            jnp.dot(block[:, :width_a], woa[...], preferred_element_type=F32)
            + jnp.dot(block[:, width_a:], wob[...], preferred_element_type=F32)
        ).astype(BF16)
        if d > 0:
            rs_copy(d).start()

    def w_tick(s, carry):
        tick(w_copy, s)
        return carry

    lax.fori_loop(2, 4, w_tick, 0)

    mine = pl.ds(pl.multiple_of(tp * own, own), own)
    total = part[mine, :].astype(F32)
    for d in range(1, tp_n):
        rs_copy(d).wait_recv()
        total = total + rs_in[d - 1].astype(F32)
    middle = x_ref[...].astype(F32) + total
    mid[...] = middle
    normed = middle * lax.rsqrt(jnp.mean(middle * middle, axis=-1, keepdims=True) + norm_eps)
    nrm[mine, :] = (normed * gmid_ref[...]).astype(BF16)

    def ag_copy(d):
        return remote(
            nrm.at[mine], nrm.at[mine], ag_send.at[d - 1], ag_recv.at[d - 1],
            tp=lax.rem(tp + d, tp_n),
        )

    for d in range(1, tp_n):
        ag_copy(d).start()
    lax.fori_loop(4, 6, w_tick, 0)
    for d in range(1, tp_n):
        ag_copy(d).wait_recv()

    chunk = wg.shape[1]

    def columns(p, width):
        return pl.ds(pl.multiple_of(at(p) * width, width), width)

    def gate_up(s):
        acc_g[...] += jnp.dot(nrm[:, columns(pos - s, chunk)], wg[s], preferred_element_type=F32)
        acc_u[...] += jnp.dot(nrm[:, columns(pos + s, chunk)], wu[s], preferred_element_type=F32)

    acc_g[...] = jnp.zeros_like(acc_g)
    acc_u[...] = jnp.zeros_like(acc_u)

    def w_caught_up(s, carry):
        gate_up(s)
        return carry

    def w_step(s, carry):
        tick(w_copy, s)
        gate_up(s)
        return carry

    lax.fori_loop(0, 4, w_caught_up, 0)
    lax.fori_loop(6, n - 1, w_step, 0)
    lax.fori_loop(4, 6, w_caught_up, 0)
    tick(w_copy, n - 1, following=d_copy)
    gate_up(n - 1)

    width = acc_g.shape[1]
    joined[:, :width] = acc_g[...].astype(BF16)
    joined[:, width:] = acc_u[...].astype(BF16)
    edge = halo_lo.shape[0]
    up_copy = remote(
        joined.at[pl.ds(rows - edge, edge)], halo_lo, h_send.at[0], h_recv.at[0], sp=above
    )
    down_copy = remote(joined.at[pl.ds(0, edge)], halo_hi, h_send.at[1], h_recv.at[1], sp=below)
    up_copy.start()
    down_copy.start()

    tick(d_copy, 2)
    up_copy.wait_recv()
    down_copy.wait_recv()
    has_low = jnp.where(sp > 0, F32(1.0), F32(0.0))
    has_high = jnp.where(sp < n - 1, F32(1.0), F32(0.0))

    def convolved(start, taps_ref):
        cut = slice(start, start + width)
        now = joined[:, cut].astype(F32)
        low = halo_lo[:, cut].astype(F32)[edge - 1:edge] * has_low
        high = halo_hi[:, cut].astype(F32)[0:1] * has_high
        line = lax.broadcasted_iota(jnp.int32, now.shape, 0)
        before = jnp.where(line == 0, low, pltpu.roll(now, 1, 0))
        after = jnp.where(line == rows - 1, high, pltpu.roll(now, rows - 1, 0))
        taps = taps_ref[...]
        return before * taps[0:1] + now * taps[1:2] + after * taps[2:3]

    gate = convolved(0, cg_ref)
    acc_g[...] = gate / (1.0 + jnp.exp(-gate))
    tick(d_copy, 3)
    hidden[...] = (acc_g[...] * convolved(width, cu_ref)).astype(BF16)

    dcols = wdr.shape[2]
    split = wdr.shape[1]
    acc_d[...] = jnp.zeros_like(acc_d)

    def down(s):
        acc_d[at(pos - s)] += jnp.dot(hidden[:, :split], wdr[s], preferred_element_type=F32)
        acc_d[at(pos + s)] += jnp.dot(hidden[:, split:], wdl[s], preferred_element_type=F32)

    def r2_copy(r, d):
        block = at(pos - r)
        to = lax.rem(tp + d, tp_n)
        return remote(
            part2.at[block, pl.ds(pl.multiple_of(to * own, own), own)], rs2_in.at[d - 1, block],
            r2_send.at[r, d - 1], r2_recv.at[r, d - 1], tp=to,
        )

    def give(r):
        block = at(pos - r)
        part2[block] = acc_d[block].astype(BF16)
        for d in range(1, tp_n):
            r2_copy(r, d).start()

    def d_caught_up(s, carry):
        down(s)
        return carry

    def d_step(s, carry):
        tick(d_copy, s)
        down(s)
        return carry

    def d_step_give(s, carry):
        tick(d_copy, s)
        down(s)
        give(s)
        give(n - s)
        return carry

    lax.fori_loop(0, 4, d_caught_up, 0)
    lax.fori_loop(4, half, d_step, 0)
    give(0)
    tick(d_copy, half)
    down(half)
    give(half)
    lax.fori_loop(half + 1, n - 1, d_step_give, 0)
    tick(d_copy, n - 1, following="end")
    down(n - 1)
    give(n - 1)
    give(1)

    def sent_r(s, carry):
        kv_r(s).wait_send()
        return carry

    def sent_l(s, carry):
        kv_l(s).wait_send()
        return carry

    def sent_w(s, carry):
        for p in range(PIECES):
            for direction in range(2):
                w_copy(s, p, direction).wait_send()
                d_copy(s, p, direction).wait_send()
        return carry

    lax.fori_loop(1, half + 1, sent_r, 0)
    lax.fori_loop(1, half, sent_l, 0)
    lax.fori_loop(1, n, sent_w, 0)
    up_copy.wait_send()
    down_copy.wait_send()
    for d in range(1, tp_n):
        rs_copy(d).wait_send()
        ag_copy(d).wait_send()

    def arrived(r, carry):
        for d in range(1, tp_n):
            r2_copy(r, d).wait_send()
            r2_copy(r, d).wait_recv()
        return carry

    lax.fori_loop(0, n, arrived, 0)
    for block in range(n):
        cut = slice(block * dcols, (block + 1) * dcols)
        summed = part2[block, mine].astype(F32)
        for d in range(1, tp_n):
            summed = summed + rs2_in[d - 1, block].astype(F32)
        out_ref[:, cut] = (mid[:, cut] + summed).astype(out_ref.dtype)


def on_device(n, tp_n, *args):
    if n % 2 or n < 8 or args[14].shape[0] % 128 or args[18].shape[1] % 128:
        return on_device_narrow(*args)
    (x_res, q_a, k_a, v_a, q_b, k_b, v_b, gain_qa, gain_ka, gain_qb, gain_kb, w_out_a, w_out_b,
     gain_mid, w_gate, w_up, conv_gate, conv_up, w_down) = args
    rows = q_a.shape[0]
    own, width = x_res.shape
    ff = w_gate.shape[1]
    heads_a, heads_b = q_a.shape[1] // DHA, q_b.shape[1] // DHB
    freq_a, freq_b = lane_frequencies(DHA, 2 * DHA), lane_frequencies(DHB, DHB)
    vmem = pl.BlockSpec(memory_space=pltpu.VMEM)
    hbm = pl.BlockSpec(memory_space=pltpu.MemorySpace.HBM)
    edge = 16
    kv_width = 2 * k_a.shape[1] + 2 * k_b.shape[1]
    dma = pltpu.SemaphoreType.DMA
    scratch = [
        pltpu.VMEM(k_a.shape, BF16),
        pltpu.VMEM(v_a.shape, BF16),
        pltpu.VMEM((n, rows, kv_width), BF16),
        pltpu.VMEM((heads_a, rows, DHA), BF16),
        pltpu.VMEM((heads_b, rows, DHB), BF16),
        pltpu.VMEM((heads_a, rows, 1), F32),
        pltpu.VMEM((heads_a, rows, 1), F32),
        pltpu.VMEM((heads_a, rows, DHA), F32),
        pltpu.VMEM((heads_b, rows, 1), F32),
        pltpu.VMEM((heads_b, rows, 1), F32),
        pltpu.VMEM((heads_b, rows, DHB), F32),
        pltpu.VMEM(w_out_a.shape, BF16),
        pltpu.VMEM(w_out_b.shape, BF16),
        pltpu.VMEM((n,) + w_gate.shape, BF16),
        pltpu.VMEM((n,) + w_up.shape, BF16),
        pltpu.VMEM((n, ff // 2, w_down.shape[1]), BF16),
        pltpu.VMEM((n, ff // 2, w_down.shape[1]), BF16),
        pltpu.VMEM((rows, q_a.shape[1] + q_b.shape[1]), BF16),
        pltpu.VMEM((rows, width), BF16),
        pltpu.VMEM((tp_n - 1, own, width), BF16),
        pltpu.VMEM((own, width), F32),
        pltpu.VMEM((rows, width), BF16),
        pltpu.VMEM((rows, ff), F32),
        pltpu.VMEM((rows, ff), F32),
        pltpu.VMEM((rows, 2 * ff), BF16),
        pltpu.VMEM((edge, 2 * ff), BF16),
        pltpu.VMEM((edge, 2 * ff), BF16),
        pltpu.VMEM((rows, ff), BF16),
        pltpu.VMEM((n, rows, w_down.shape[1]), F32),
        pltpu.VMEM((n, rows, w_down.shape[1]), BF16),
        pltpu.VMEM((tp_n - 1, n, own, w_down.shape[1]), BF16),
        dma((8,)),
        dma((n,)), dma((n,)),
        dma((2, PIECES, n)), dma((2, PIECES, n)),
        dma((2, PIECES, n)), dma((2, PIECES, n)),
        dma((tp_n - 1,)), dma((tp_n - 1,)),
        dma((tp_n - 1,)), dma((tp_n - 1,)),
        dma((2,)), dma((2,)),
        dma((n, tp_n - 1)), dma((n, tp_n - 1)),
    ]
    return pl.pallas_call(
        functools.partial(kernel, n, tp_n),
        out_shape=jax.ShapeDtypeStruct(x_res.shape, BF16),
        in_specs=[vmem] * 2 + [hbm] * 2 + [vmem] * 9 + [hbm, hbm, vmem, hbm, hbm, vmem, vmem, hbm],
        out_specs=vmem,
        scratch_shapes=scratch,
        compiler_params=pltpu.CompilerParams(
            collective_id=0, has_side_effects=True, vmem_limit_bytes=60 * 1024 * 1024
        ),
        name="layer",
    )(
        x_res, q_a, k_a, v_a, q_b, k_b, v_b,
        gain_qa[None], gain_ka[None], gain_qb[None], gain_kb[None],
        freq_a, freq_b,
        w_out_a, w_out_b, gain_mid[None], w_gate, w_up, conv_gate, conv_up, w_down,
    )


def extended(block, sides, width):
    for axis, dim in sides:
        count = lax.axis_size(axis)
        forward = [(i, i + 1) for i in range(count - 1)]
        backward = [(target, source) for source, target in forward]
        low = lax.ppermute(
            lax.slice_in_dim(block, block.shape[dim] - width, None, axis=dim), axis, forward
        )
        high = lax.ppermute(lax.slice_in_dim(block, 0, width, axis=dim), axis, backward)
        block = jnp.concatenate([low, block, high], axis=dim)
    return block


def rotate_half(values):
    first, second = jnp.split(values, 2, axis=-1)
    return jnp.concatenate([-second, first], axis=-1)


def prepare(raw, gain, head_size, positions):
    count = raw.shape[0]
    heads = raw.shape[1] // head_size
    values = raw.astype(jnp.float32).reshape(count, heads, head_size)
    values = values * lax.rsqrt(jnp.mean(values * values, axis=-1, keepdims=True) + norm_eps)
    values = values * gain
    angles = rotary_angles(positions, head_size)
    cosine, sine = jnp.cos(angles), jnp.sin(angles)
    row_part, col_part = jnp.split(values, 2, axis=-1)
    turned = jnp.concatenate([rotate_half(row_part), rotate_half(col_part)], axis=-1)
    values = values * cosine[:, None, :] + turned * sine[:, None, :]
    return values.astype(jnp.bfloat16)


def start_state(queries):
    count, kv_heads, groups, head_size = queries.shape
    lowest = jnp.full((kv_heads, groups, count), -1e30, jnp.float32)
    totals = jnp.zeros((kv_heads, groups, count), jnp.float32)
    summed = jnp.zeros((kv_heads, groups, count, head_size), jnp.float32)
    return (lowest, totals, summed)


def attend(state, queries, key_piece, value_piece):
    head_size = queries.shape[3]
    kv_heads = queries.shape[1]
    length = key_piece.shape[0]
    keys = key_piece.reshape(length, kv_heads, head_size)
    values = value_piece.reshape(length, kv_heads, head_size)
    span = length
    while span > 1024 and span % 2 == 0:
        span = span // 2
    scale = jnp.float32(head_size ** (-0.5))

    def one_span(index, carry):
        running, totals, summed = carry
        key_rows = lax.dynamic_slice_in_dim(keys, index * span, span, 0)
        value_rows = lax.dynamic_slice_in_dim(values, index * span, span, 0)
        scores = (
            jnp.einsum("qkgd,skd->kgqs", queries, key_rows, preferred_element_type=jnp.float32)
            * scale
        )
        highest = jnp.maximum(running, jnp.max(scores, axis=-1))
        factor = jnp.exp(running - highest)
        expd = jnp.exp(scores - highest[..., None])
        totals = totals * factor + jnp.sum(expd, axis=-1)
        summed = summed * factor[..., None] + jnp.einsum(
            "kgqs,skd->kgqd",
            expd.astype(jnp.bfloat16),
            value_rows,
            preferred_element_type=jnp.float32,
        )
        return (highest, totals, summed)

    return lax.fori_loop(0, length // span, one_span, state)


def finish(state):
    running, totals, summed = state
    kv_heads, groups, count, head_size = summed.shape
    result = summed / totals[..., None]
    return (
        jnp.transpose(result, (2, 0, 1, 3))
        .reshape(count, kv_heads * groups * head_size)
        .astype(jnp.bfloat16)
    )


def on_device_narrow(
    x_res,
    q_a,
    k_a,
    v_a,
    q_b,
    k_b,
    v_b,
    gain_qa,
    gain_ka,
    gain_qb,
    gain_kb,
    w_out_a,
    w_out_b,
    gain_mid,
    w_gate,
    w_up,
    conv_gate,
    conv_up,
    w_down,
):
    tok_rows = q_a.shape[0]
    whole_gate, whole_up, whole_down = (
        lax.all_gather(w_gate, "sp", axis=0, tiled=True),
        lax.all_gather(w_up, "sp", axis=0, tiled=True),
        lax.all_gather(w_down, "sp", axis=1, tiled=True),
    )
    positions = lax.axis_index("sp") * tok_rows + lax.iota(jnp.int32, tok_rows)
    kv_a = k_a.shape[1] // DHA
    kv_b = k_b.shape[1] // DHB
    query_a = prepare(q_a, gain_qa, DHA, positions)
    query_a = query_a.reshape(tok_rows, kv_a, query_a.shape[1] // kv_a, DHA)
    query_b = prepare(q_b, gain_qb, DHB, positions)
    query_b = query_b.reshape(tok_rows, kv_b, query_b.shape[1] // kv_b, DHB)
    keys_a = prepare(k_a, gain_ka, DHA, positions).reshape(tok_rows, kv_a * DHA)
    keys_b = prepare(k_b, gain_kb, DHB, positions).reshape(tok_rows, kv_b * DHB)
    state_a = attend(
        start_state(query_a),
        query_a,
        lax.all_gather(keys_a, "sp", axis=0, tiled=True),
        lax.all_gather(v_a, "sp", axis=0, tiled=True),
    )
    state_b = attend(
        start_state(query_b),
        query_b,
        lax.all_gather(keys_b, "sp", axis=0, tiled=True),
        lax.all_gather(v_b, "sp", axis=0, tiled=True),
    )
    attn_a = finish(state_a)
    attn_b = finish(state_b)
    projected = lax.psum_scatter(
        (
            jnp.dot(attn_a, w_out_a, preferred_element_type=jnp.float32)
            + jnp.dot(attn_b, w_out_b, preferred_element_type=jnp.float32)
        ).astype(jnp.bfloat16),
        "tp",
        scatter_dimension=0,
        tiled=True,
    ).astype(jnp.float32)
    middle = x_res.astype(jnp.float32) + projected
    normed = middle * lax.rsqrt(jnp.mean(middle * middle, axis=-1, keepdims=True) + norm_eps)
    normed = (normed * gain_mid).astype(jnp.bfloat16)
    gathered = lax.all_gather(normed, "tp", axis=0, tiled=True)
    gate_pre = jnp.dot(gathered, whole_gate, preferred_element_type=jnp.float32)
    up_pre = jnp.dot(gathered, whole_up, preferred_element_type=jnp.float32)
    width = gate_pre.shape[1]
    joined = jnp.concatenate([gate_pre, up_pre], axis=1).astype(jnp.bfloat16)
    padded = extended(joined, (("sp", 0),), 1)
    taps = jnp.concatenate([conv_gate, conv_up], axis=1)
    mixed = padded[:-2] * taps[0] + padded[1:-1] * taps[1] + padded[2:] * taps[2]
    hidden = (jax.nn.silu(mixed[:, :width]) * mixed[:, width:]).astype(jnp.bfloat16)
    terms = jnp.dot(hidden, whole_down, preferred_element_type=jnp.float32)
    summed = lax.psum_scatter(
        terms.astype(jnp.bfloat16), "tp", scatter_dimension=0, tiled=True
    ).astype(jnp.float32)
    return (middle + summed).astype(jnp.bfloat16)


def solution(mesh):
    in_specs = (
        P(("sp", "tp"), None),
        P("sp", "tp"),
        P("sp", "tp"),
        P("sp", "tp"),
        P("sp", "tp"),
        P("sp", "tp"),
        P("sp", "tp"),
        P(),
        P(),
        P(),
        P(),
        P("tp", None),
        P("tp", None),
        P(),
        P("sp", "tp"),
        P("sp", "tp"),
        P(None, "tp"),
        P(None, "tp"),
        P("tp", "sp"),
    )
    out_specs = P(("sp", "tp"), None)
    body = functools.partial(on_device, mesh.shape["sp"], mesh.shape["tp"])
    return jax.shard_map(
        body, mesh=mesh, in_specs=in_specs, out_specs=out_specs, check_vma=False
    )
```

profile of v0, /device:TPU:0, one launch (start us, length us, event | category | flops | bytes accessed | tf_op | source)
XLA Modules:
  0.0 129.7 jit_solution(12662845667053300418)
XLA Ops:
  0.0 0.6 broadcast_in_dim_tile.7.frb_ref
  0.7 0.6 broadcast_in_dim_tile.6.fra_ref
  1.2 0.0 copy-start
  1.2 1.5 %copy.20.ka_hbm = bf16[256,64]{1,0:T(8,128)(2,1)} copy(bf16[256,64]{0,1:T(8,128)(2,1)} %param.21) | data formatting | bytes 65536 | tf_op args[2]
  2.7 0.0 copy-done
  2.7 0.7 copy.21.va_hbm
  3.5 124.6 %layer.1 = bf16[64,2048]{1,0:T(8,128)(2,1)} custom-call(bf16[64,2048]{1,0:T(8,128)(2,1)} %x_ref.1, bf16[256,256]{1,0:T(8,128)(2,1)} %qa_ref.1, bf16[256,64]{1,0:T(8,128)(2,1)} %copy.20.ka_hbm, bf16[256,64]{1,0:T(8,128)(2,1)} %copy.21.va_hbm, bf16[256,256]{1,0:T(8,128)(2,1)} %qb_ref.1, bf16[256,128]{1,0:T(8,128)(2,1)} %kb_ref.1, bf16[256,128]{1,0:T(8,128)(2,1)} %vb_ref.1, ...), custom_call_target="tpu_custom_call" | custom-call | tf_op jit(solution)/shard_map/layer/pallas_call | solution.py:545
  128.1 1.7 %copy.23 = bf16[64,2048]{1,0:T(8,128)(2,1)} copy(bf16[64,2048]{1,0:T(8,128)(2,1)} %layer.1) | data formatting | bytes 524288
  (4 shorter events, 0.0 us)
Async XLA Ops:
  1.2 1.5 %copy-start = (bf16[256,64]{0,1:T(8,128)(2,1)S(1)}, bf16[256,64]{0,1:T(8,128)(2,1)}, u32[]{:S(2)}) copy-start(bf16[256,64]{0,1:T(8,128)(2,1)} %param.22) | copy-start | bytes 98308
where the time goes:
time: 130 us
  Pallas kernels  125 us (96%)
  local copies, waits for them, and re-layouts  5.11 us (4%)
    pallas_call x1, Pallas kernels, on_device(): pl.pallas_call(functools.partial(kernel, n, tp_n), out_shape=jax.ShapeDty...  125 us
    unnamed x5, local copies, waits for them, and re-layouts  3.9 us

commit v1 on v0

v1 whole, which is shorter than its diff:
```python
import functools

import jax
import jax.numpy as jnp
import numpy as np
from jax import lax
from jax.experimental import pallas as pl
from jax.experimental.pallas import tpu as pltpu
from jax.sharding import PartitionSpec as P

DHA = 64
DHB = 128

norm_eps = 1e-06
rope_theta = 10000.0
F32 = jnp.float32
BF16 = jnp.bfloat16
MESH = pl.DeviceIdType.MESH
GU_PIECES = 4
DN_PIECES = 2


def rotary_angles(positions, head_size):
    half = head_size // 2
    inverse = jnp.power(jnp.float32(rope_theta), -jnp.arange(0, half, 2, dtype=jnp.float32) / half)
    grid_row = (positions // 64).astype(jnp.float32)[:, None] * inverse[None, :]
    grid_col = (positions % 64).astype(jnp.float32)[:, None] * inverse[None, :]
    return jnp.concatenate([grid_row, grid_row, grid_col, grid_col], axis=-1)


def lane_frequencies(head_size, width):
    half = head_size // 2
    steps = -np.arange(0, half, 2, dtype=np.float32) / np.float32(half)
    inverse = np.power(np.float32(rope_theta), steps).astype(np.float32)
    return jnp.asarray(np.tile(inverse, width // inverse.shape[0])[None])


def block_mean(width, head):
    i = lax.broadcasted_iota(jnp.int32, (width, width), 0)
    j = lax.broadcasted_iota(jnp.int32, (width, width), 1)
    return jnp.where(lax.div(i, head) == lax.div(j, head), F32(1.0 / head), F32(0.0))


def block_turn(width, head):
    quarter = head // 4
    i = lax.broadcasted_iota(jnp.int32, (width, width), 0)
    j = lax.broadcasted_iota(jnp.int32, (width, width), 1)
    first = lax.rem(j, 2 * quarter) < quarter
    return jnp.where(
        first & (i == j + quarter),
        F32(-1.0),
        jnp.where(jnp.logical_not(first) & (i == j - quarter), F32(1.0), F32(0.0)),
    )


def exact_dot(a, b):
    return jnp.dot(a, b, precision=lax.Precision.HIGHEST, preferred_element_type=F32)


def prepared(raw, gain, angle_cos, angle_sin, head):
    width = raw.shape[1]
    values = raw.astype(F32)
    values = values * lax.rsqrt(exact_dot(values * values, block_mean(width, head)) + norm_eps)
    values = values * gain
    turned = exact_dot(values, block_turn(width, head))
    return (values * angle_cos + turned * angle_sin).astype(BF16)


def kernel(
    x_ref, qa_ref, kat_ref, vat_ref, qb_ref, kb_ref, vb_ref,
    gqa_ref, gka_ref, gqb_ref, gkb_ref,
    fra_ref, frb_ref,
    woa_hbm, wob_hbm, gmid_ref, wg_hbm, wu_hbm, cg_ref, cu_ref, wd_hbm,
    out_ref,
    kv, qas, qbs, m_a, l_a, acc_a, m_b, l_b, acc_b,
    woa, wob, gub, gux, dnb, dnx,
    attn, pout, own1, s1_in, q1, s2_in, mid, nrm, acc, eg_out, eg_x, eg_p, hid,
    p2, own2, s2a, q2, s2b,
    loc_sem, kvz_s, kvz_r, kvx_s, kvx_r, guz_s, guz_r, gux_s, gux_r,
    dnz_s, dnz_r, dnx_s, dnx_r, s1_s, s1_r, s2_s, s2_r,
    agz_s, agz_r, agy_s, agy_r, agf_s, agf_r, agc_s, agc_r, eg_s, eg_r,
    d1_s, d1_r, d2_s, d2_r,
):
    sp = lax.axis_index("sp")
    tp = lax.axis_index("tp")
    z, x = lax.div(sp, 2), lax.rem(sp, 2)
    y, c = lax.div(tp, 2), lax.rem(tp, 2)
    rows = qa_ref.shape[0]
    own = x_ref.shape[0]
    chunk, ff = gub.shape[2], gub.shape[3] // 2
    flip = lax.div(z, 2)

    def mz(v):
        return (1 - flip) * v + flip * (3 - v)

    u = mz(z)
    inner, end = u == 1, u == 0
    mate = mz(1 - u)
    my_h = lax.rem(z, 2)
    jz = my_h
    h_end, h_in = lax.rem(mz(0), 2), lax.rem(mz(1), 2)
    cross = lax.rem(x + flip, 2)
    far = 2 * (1 - flip) * 2 - 2 + z
    twin = 1 - u
    ranks = [u, twin, 2, 3]

    def tp_at(yy, cc):
        return yy * 2 + cc

    barrier = pltpu.get_barrier_semaphore()
    greet = [
        (None, {"sp": 2 * z + 1 - x}),
        (None, {"tp": tp_at(y, 1 - c)}),
        (None, {"tp": tp_at(1 - y, c)}),
        (None, {"sp": 2 * mate + x}),
        (None, {"sp": 2 * mate + x, "tp": tp_at(1 - y, c)}),
        (inner, {"sp": 2 * mz(2) + x}),
        (cross == 1, {"sp": 2 * far + 1 - x}),
    ]
    for cond, where in greet:
        def signal(where=where):
            pl.semaphore_signal(barrier, inc=1, device_id=where, device_id_type=MESH)
        if cond is None:
            signal()
        else:
            pl.when(cond)(signal)

    loc = []
    for h in range(2):
        cut = pl.ds(h * ff, ff)
        loc.append(pltpu.make_async_copy(
            wg_hbm.at[:, cut], gub.at[z, h, :, pl.ds(0, ff)], loc_sem.at[len(loc)]))
        loc.append(pltpu.make_async_copy(
            wu_hbm.at[:, cut], gub.at[z, h, :, pl.ds(ff, ff)], loc_sem.at[len(loc)]))
    for h in range(2):
        loc.append(pltpu.make_async_copy(
            wd_hbm.at[pl.ds(h * ff, ff)], dnb.at[z, h], loc_sem.at[len(loc)]))
    loc.append(pltpu.make_async_copy(woa_hbm, woa, loc_sem.at[len(loc)]))
    loc.append(pltpu.make_async_copy(wob_hbm, wob, loc_sem.at[len(loc)]))
    for copy in loc:
        copy.start()

    def remote(src, dst, send, recv, **where):
        return pltpu.make_async_remote_copy(
            src_ref=src, dst_ref=dst, send_sem=send, recv_sem=recv,
            device_id=where, device_id_type=MESH,
        )

    sent = []

    def under(cond, run):
        if cond is None:
            run()
        else:
            pl.when(cond)(run)

    def go(cond, copies):
        def run():
            for copy in copies:
                copy().start()
        under(cond, run)
        sent.append((cond, copies))

    def got(cond, copies):
        def run():
            for copy in copies:
                copy().wait_recv()
        under(cond, run)

    P = functools.partial
    gr, dr = chunk // GU_PIECES, ff // DN_PIECES
    everyp, everyd = range(GU_PIECES), range(DN_PIECES)

    def kv_z(vb, to, way):
        zi = mz(vb)
        return remote(kv.at[0, zi], kv.at[0, zi], kvz_s.at[way, zi], kvz_r.at[zi], sp=2 * mz(to) + x)

    def kv_x(vb):
        zi = mz(vb)
        return remote(kv.at[0, zi], kv.at[1, zi], kvx_s.at[zi], kvx_r.at[zi], sp=2 * z + 1 - x)

    def gu_z(vb, h, p, to, way):
        zi, cut = mz(vb), pl.ds(p * gr, gr)
        return remote(
            gub.at[zi, h, cut], gub.at[zi, h, cut],
            guz_s.at[way, zi, h, p], guz_r.at[zi, h, p], sp=2 * mz(to) + x,
        )

    def gu_x(vb, p):
        zi, cut = mz(vb), pl.ds(p * gr, gr)
        return remote(
            gub.at[zi, my_h, cut], gux.at[zi, cut],
            gux_s.at[zi, p], gux_r.at[zi, p], sp=2 * z + 1 - x,
        )

    def dn_z(vb, h, p, to, way):
        zi, cut = mz(vb), pl.ds(p * dr, dr)
        return remote(
            dnb.at[zi, h, cut], dnb.at[zi, h, cut],
            dnz_s.at[way, zi, h, p], dnz_r.at[zi, h, p], sp=2 * mz(to) + x,
        )

    def dn_x(vb, p):
        zi, cut = mz(vb), pl.ds(p * dr, dr)
        return remote(
            dnb.at[zi, my_h, cut], dnx.at[zi, cut],
            dnx_s.at[zi, p], dnx_r.at[zi, p], sp=2 * z + 1 - x,
        )

    def gu_to(vb, h, to, way, pieces=everyp):
        return [P(gu_z, vb, h, p, to, way) for p in pieces]

    def dn_to(vb, h, to, way):
        return [P(dn_z, vb, h, p, to, way) for p in everyd]

    def gu_over(vb, pieces=everyp):
        return [P(gu_x, vb, p) for p in pieces]

    def dn_over(vb):
        return [P(dn_x, vb, p) for p in everyd]

    def gu_in(vb, h):
        return [P(gu_z, vb, h, p, 1 - u, 0) for p in everyp]

    def dn_in(vb, h):
        return [P(dn_z, vb, h, p, 1 - u, 0) for p in everyd]

    def kv_in(vb):
        return [P(kv_z, vb, 1 - u, 0)]

    for copy in loc[:4]:
        copy.wait()
    pl.semaphore_wait(barrier, 5 + u + cross)
    go(inner, gu_to(u, h_in, 2, 0, [0]))
    go(inner, gu_to(u, h_end, 0, 1, [0]))
    go(end, gu_to(u, h_in, 1, 0, [0]))
    go(None, gu_over(u, [0]))

    def tables(freq_ref, head):
        shape = (rows, freq_ref.shape[1])
        token = lax.broadcasted_iota(jnp.int32, shape, 0) + sp * rows
        lane = lax.broadcasted_iota(jnp.int32, shape, 1)
        grid = jnp.where(lax.rem(lane, head) < head // 2, lax.div(token, 64), lax.rem(token, 64))
        angles = grid.astype(F32) * freq_ref[...]
        return jnp.cos(angles), jnp.sin(angles)

    ca, sa = tables(fra_ref, DHA)
    cb, sb = tables(frb_ref, DHB)
    wka, wkb = kat_ref.shape[0], kb_ref.shape[1]

    def wide(table, width):
        if width <= table.shape[1]:
            return table[:, :width]
        return jnp.concatenate([table] * (width // table.shape[1]), axis=1)

    def gains(ref, width):
        g = ref[...]
        count = width // g.shape[1]
        return g if count == 1 else jnp.concatenate([g] * count, axis=1)

    raw_a = jnp.transpose(kat_ref[...].astype(F32))
    val_a = jnp.transpose(vat_ref[...].astype(F32)).astype(BF16)
    keys_a = prepared(raw_a, gains(gka_ref, wka), wide(ca, wka), wide(sa, wka), DHA)
    keys_b = prepared(kb_ref[...], gains(gkb_ref, wkb), wide(cb, wkb), wide(sb, wkb), DHB)
    kv[0, z, :, :wkb] = keys_b
    kv[0, z, :, wkb:2 * wkb] = vb_ref[...]
    kv[0, z, :, 2 * wkb:] = jnp.concatenate([keys_a, val_a], axis=1)

    go(inner, [P(kv_z, u, 2, 0), P(kv_z, u, 0, 1)])
    go(end, [P(kv_z, u, 1, 0)])
    go(None, [P(kv_x, u)])
    go(inner, gu_to(u, h_in, 2, 0, [1]) + gu_to(u, h_end, 0, 1, [1]))
    go(end, gu_to(u, h_in, 1, 0, everyp[1:]) + gu_to(u, h_end, 1, 0))
    go(None, gu_over(u, [1]))
    for copy in loc[4:]:
        copy.wait()
    go(end, dn_to(u, h_in, 1, 0) + dn_to(u, h_end, 1, 0))

    heads_a = qa_ref.shape[1] // DHA
    heads_b = qb_ref.shape[1] // DHB
    qa = prepared(
        qa_ref[...], gains(gqa_ref, heads_a * DHA), wide(ca, heads_a * DHA),
        wide(sa, heads_a * DHA), DHA,
    )
    qb = prepared(
        qb_ref[...], gains(gqb_ref, heads_b * DHB), wide(cb, heads_b * DHB),
        wide(sb, heads_b * DHB), DHB,
    )
    for h in range(heads_a):
        qas[h] = qa[:, h * DHA:(h + 1) * DHA]
    for h in range(heads_b):
        qbs[h] = qb[:, h * DHB:(h + 1) * DHB]
    for ref, low in ((m_a, -1e30), (m_b, -1e30), (l_a, 0.0), (l_b, 0.0), (acc_a, 0.0), (acc_b, 0.0)):
        ref[...] = jnp.full(ref.shape, low, F32)

    def attend_one(queries, key_rows, value_rows, m, l, total, h):
        scale = F32(queries.shape[2] ** (-0.5))
        scores = lax.dot_general(
            queries[h], key_rows, (((1,), (1,)), ((), ())), preferred_element_type=F32
        ) * scale
        before = m[h]
        highest = jnp.maximum(before, jnp.max(scores, axis=-1, keepdims=True))
        factor = jnp.exp(before - highest)
        expd = jnp.exp(scores - highest)
        l[h] = l[h] * factor + jnp.sum(expd, axis=-1, keepdims=True)
        total[h] = total[h] * factor + jnp.dot(
            expd.astype(BF16), value_rows, preferred_element_type=F32
        )
        m[h] = highest

    def attend(col, zi):
        for h in range(heads_b):
            attend_one(
                qbs, kv[col, zi, :, :wkb], kv[col, zi, :, wkb:2 * wkb], m_b, l_b, acc_b, h
            )
        pair = kv[col, zi, :, 2 * wkb:]
        for h in range(heads_a):
            attend_one(qas, pair[:, :wka], pair[:, wka:], m_a, l_a, acc_a, h)

    def rank(k):
        high = k // 2 if isinstance(k, int) else lax.div(k, 2)
        return mz(high * k + (1 - high) * (k + u - 2 * k * u))

    attend(0, z)

    def kv_crossed(zi):
        remote(
            kv.at[0, zi], kv.at[1, zi], kvx_s.at[zi], kvx_r.at[zi], sp=2 * z + 1 - x
        ).wait_recv()

    def attend_step(i, carry):
        @pl.when(i == 1)
        def _():
            got(None, kv_in(twin))
            go(inner, [P(kv_z, 0, 2, 0)])
            go(None, [P(kv_x, twin)])
            got(inner, kv_in(2))
            go(inner, [P(kv_z, 2, 0, 1), P(kv_x, 2)])
            go(inner, gu_to(u, h_in, 2, 0, everyp[2:]) + gu_to(u, h_end, 2, 0))
            go(inner, gu_to(u, h_end, 0, 1, [2]))
            go(end, gu_over(u, [2]))

        @pl.when(i == 2)
        def _():
            got(end, kv_in(2))
            go(end, [P(kv_x, 2)])
            got(inner, kv_in(3))
            go(inner, [P(kv_z, 3, 0, 1), P(kv_x, 3)])
            go(inner, gu_to(u, h_end, 0, 1, everyp[3:]))
            go(inner, gu_over(u, [2]))

        @pl.when(i == 3)
        def _():
            got(end, kv_in(3))
            go(end, [P(kv_x, 3)])
            go(None, gu_over(u, everyp[3:]))
            got(inner, gu_in(2, h_end))
            go(inner, gu_to(2, h_end, 0, 1))
            got(inner, gu_in(0, h_in))
            go(inner, gu_to(0, h_in, 2, 0))

        attend(0, rank(i))

        @pl.when(i == 3)
        def _():
            got(end, gu_in(1, my_h))
            go(None, gu_over(twin))
            got(inner, gu_in(0, h_end))
            go(inner, gu_to(0, h_end, 2, 0))
            go(inner, dn_to(u, h_in, 2, 0) + dn_to(u, h_end, 2, 0))

        back = rank(i - 1)
        kv_crossed(back)
        attend(1, back)
        return carry

    lax.fori_loop(1, 4, attend_step, 0)
    kv_crossed(rank(3))
    attend(1, rank(3))

    for h in range(heads_a):
        attn[:, h * DHA:(h + 1) * DHA] = (acc_a[h] / l_a[h]).astype(BF16)
    width_a = heads_a * DHA
    for h in range(heads_b):
        attn[:, width_a + h * DHB:width_a + (h + 1) * DHB] = (acc_b[h] / l_b[h]).astype(BF16)

    def s1_copy(k):
        yy = (1 - y, y)[k]
        return remote(
            pout.at[yy], s1_in.at[yy], s1_s.at[k], s1_r.at[k], tp=tp_at(y, 1 - c)
        )

    def s2_copy():
        return remote(q1, s2_in, s2_s.at[0], s2_r.at[0], tp=tp_at(1 - y, c))

    for who, cc in enumerate((1 - c, c)):
        for k, yy in enumerate((1 - y, y)):
            block = attn[pl.ds(pl.multiple_of(tp_at(yy, cc) * own, own), own), :]
            value = (
                jnp.dot(block[:, :width_a], woa[...], preferred_element_type=F32)
                + jnp.dot(block[:, width_a:], wob[...], preferred_element_type=F32)
            )
            if who == 0:
                pout[yy] = value.astype(BF16)
                go(None, [P(s1_copy, k)])
            else:
                own1[yy] = value

    got(None, [P(s1_copy, 0)])
    q1[...] = (own1[1 - y] + s1_in[1 - y].astype(F32)).astype(BF16)
    go(None, [s2_copy])

    got(None, gu_in(2, my_h))
    go(None, gu_over(2))
    go(None, dn_over(u))
    go(inner, dn_to(u, h_end, 0, 1))
    got(inner, gu_in(3, h_end))
    go(inner, gu_to(3, h_end, 0, 1))
    got(inner, dn_in(0, h_in) + dn_in(0, h_end))
    go(inner, dn_to(0, h_in, 2, 0) + dn_to(0, h_end, 2, 0))
    got(end, dn_in(1, my_h))
    go(None, dn_over(1 - u))

    mine = pl.ds(pl.multiple_of(tp * own, own), own)
    got(None, [P(s1_copy, 1)])
    middle = x_ref[...].astype(F32) + own1[y] + s1_in[y].astype(F32)
    got(None, [s2_copy])
    middle = middle + s2_in[...].astype(F32)
    mid[...] = middle
    normed = middle * lax.rsqrt(jnp.mean(middle * middle, axis=-1, keepdims=True) + norm_eps)
    nrm[jz, mine, :] = (normed * gmid_ref[...]).astype(BF16)

    part = own // 2

    def rows_of(tt, p=None):
        if p is None:
            return pl.ds(pl.multiple_of(tt * own, own), own)
        return pl.ds(pl.multiple_of(tt * own + p * part, part), part)

    def ag_z(p, j):
        at = nrm.at[j, rows_of(tp, p)]
        return remote(at, at, agz_s.at[p], agz_r.at[p], sp=2 * mate + x)

    def ag_y(tt):
        at = nrm.at[jz, rows_of(tt)]
        return remote(at, at, agy_s.at[0], agy_r.at[0], tp=tp_at(1 - y, c))

    def ag_f(p, tt):
        at = nrm.at[1 - jz, rows_of(tt, p)]
        return remote(at, at, agf_s.at[p], agf_r.at[p], tp=tp_at(1 - y, c))

    def ag_c(k, cc):
        j, tt = ((jz, tp_at(y, cc)), (jz, tp_at(1 - y, cc)),
                 (1 - jz, tp_at(y, cc)), (1 - jz, tp_at(1 - y, cc)))[k]
        at = nrm.at[j, rows_of(tt)]
        return remote(at, at, agc_s.at[k], agc_r.at[k], tp=tp_at(y, 1 - c))

    go(None, [P(ag_z, 0, jz), P(ag_y, tp), P(ag_z, 1, jz), P(ag_c, 0, c)])

    got(None, gu_in(3, my_h))
    go(None, gu_over(3))

    for p in range(2):
        got(None, [P(ag_z, p, 1 - jz)])
        go(None, [P(ag_f, p, tp)])
    go(None, [P(ag_c, 2, c)])
    got(None, [P(ag_y, tp_at(1 - y, c))])
    go(None, [P(ag_c, 1, c)])

    def gate_up(j, col, zi):
        side = (1 - col) * x + col * (1 - x)
        columns = pl.ds(pl.multiple_of((2 * zi + side) * chunk, chunk), chunk)
        weights = gux[zi] if col else gub[zi, my_h]
        acc[j] += jnp.dot(nrm[j, :, columns], weights, preferred_element_type=F32)

    def gu_crossed(zi):
        for p in everyp:
            cut = pl.ds(p * gr, gr)
            remote(
                gub.at[zi, my_h, cut], gux.at[zi, cut],
                gux_s.at[zi, p], gux_r.at[zi, p], sp=2 * z + 1 - x,
            ).wait_recv()

    acc[...] = jnp.zeros_like(acc)
    got(None, [P(ag_c, 0, 1 - c), P(ag_c, 1, 1 - c)])

    def near_rows(k, carry):
        zi = rank(k)
        gate_up(jz, 0, zi)
        gu_crossed(zi)
        gate_up(jz, 1, zi)
        return carry

    def other_rows(k, carry):
        zi = rank(k)
        gate_up(1 - jz, 0, zi)
        gate_up(1 - jz, 1, zi)
        return carry

    lax.fori_loop(0, 2, near_rows, 0)
    for p in range(2):
        got(None, [P(ag_f, p, tp_at(1 - y, c))])
    go(None, [P(ag_c, 3, c)])
    lax.fori_loop(2, 3, near_rows, 0)
    got(None, [P(ag_c, 2, 1 - c), P(ag_c, 3, 1 - c)])
    lax.fori_loop(0, 3, other_rows, 0)
    last = mz(3)
    gate_up(jz, 0, last)
    gate_up(1 - jz, 0, last)
    gu_crossed(last)
    gate_up(jz, 1, last)
    gate_up(1 - jz, 1, last)

    def edge_x():
        return remote(eg_out, eg_x, eg_s.at[0], eg_r.at[0], sp=2 * z + 1 - x)

    def edge_p():
        return remote(eg_out, eg_p, eg_s.at[1], eg_r.at[1], sp=2 * far + 1 - x)

    rim = [acc[j, at:at + 1, :] for j in range(2) for at in (0, rows - 1)]
    rim.append(jnp.zeros((eg_out.shape[0] - 4, 2 * ff), F32))
    eg_out[...] = jnp.concatenate(rim, axis=0).astype(BF16)
    go(None, [edge_x])
    go(cross == 1, [edge_p])

    @pl.when(cross == 0)
    def _():
        eg_p[...] = jnp.zeros_like(eg_p)

    got(inner, dn_in(2, h_end))
    go(inner, dn_to(2, h_end, 0, 1))
    got(None, dn_in(2, my_h))
    go(None, dn_over(2))

    got(None, [edge_x])
    got(cross == 1, [edge_p])

    is_right = x == 1

    def convolved(j, lane, taps_ref):
        cut = slice(lane, lane + ff)
        now = acc[j, :, cut].astype(BF16).astype(F32)
        beside = eg_x[:, cut].astype(F32)
        beyond = eg_p[:, cut].astype(F32)
        if j == 0:
            low = jnp.where(is_right, beside[1:2], beyond[3:4])
            high = jnp.where(is_right, beside[2:3], beside[0:1])
        else:
            low = jnp.where(is_right, beside[3:4], beside[1:2])
            high = jnp.where(is_right, beyond[0:1], beside[2:3])
        line = lax.broadcasted_iota(jnp.int32, now.shape, 0)
        before = jnp.where(line == 0, low, pltpu.roll(now, 1, 0))
        after = jnp.where(line == rows - 1, high, pltpu.roll(now, rows - 1, 0))
        taps = taps_ref[:, pl.ds(pl.multiple_of(my_h * ff, ff), ff)]
        return before * taps[0:1] + now * taps[1:2] + after * taps[2:3]

    for j in range(2):
        gate = convolved(j, 0, cg_ref)
        out = (gate / (1.0 + jnp.exp(-gate)) * convolved(j, ff, cu_ref)).astype(BF16)
        for yy in range(2):
            for cc in range(2):
                at = tp_at(yy, cc) * own
                to = (j * 2 + yy) * own
                hid[cc, to:to + own, :] = out[at:at + own]

    def d1_copy(b):
        return remote(p2.at[b], s2a.at[b], d1_s.at[b], d1_r.at[b], tp=tp_at(y, 1 - c))

    def d2_copy(b, k):
        jj, yy = ((jz, 1 - y), (1 - jz, y), (1 - jz, 1 - y))[k]
        where = ({"tp": tp_at(1 - y, c)}, {"sp": 2 * mate + x},
                 {"sp": 2 * mate + x, "tp": tp_at(1 - y, c)})[k]
        return remote(
            q2.at[b, 2 * jj + yy], s2b.at[b, k], d2_s.at[b, k], d2_r.at[b, k], **where
        )

    def block_of(col, vb):
        side = (1 - col) * x + col * (1 - x)
        return 2 * mz(vb) + side

    def first_sum(col, vb):
        b = block_of(col, vb)
        weights = dnx[mz(vb)] if col else dnb[mz(vb), my_h]
        p2[b] = jnp.dot(hid[1 - c], weights, preferred_element_type=F32).astype(BF16)
        go(None, [P(d1_copy, b)])
        own2[b] = jnp.dot(hid[c], weights, preferred_element_type=F32)

    def second_sum(col, vb):
        b = block_of(col, vb)
        got(None, [P(d1_copy, b)])
        value = own2[b] + s2a[b].astype(F32)
        own2[b] = value
        short = value.astype(BF16)
        for k in range(4):
            q2[b, k] = short[k * own:(k + 1) * own]
        go(None, [P(d2_copy, b, k) for k in (2, 0, 1)])

    def down(k):
        first_sum(0, ranks[k])
        got(None, dn_over(ranks[k]))
        first_sum(1, ranks[k])

    def pass_on(k):
        second_sum(0, ranks[k])
        second_sum(1, ranks[k])

    down(0)
    down(1)
    pass_on(0)
    down(2)
    pass_on(1)
    pass_on(2)
    got(inner, dn_in(3, h_end))
    go(inner, dn_to(3, h_end, 0, 1))
    got(None, dn_in(3, my_h))
    go(None, dn_over(3))
    down(3)
    pass_on(3)

    dcols = dnx.shape[2]
    here = pl.ds(pl.multiple_of((2 * jz + y) * own, own), own)

    for b in range(own2.shape[0]):
        got(None, [P(d2_copy, b, i) for i in range(3)])
        cut = slice(b * dcols, (b + 1) * dcols)
        value = own2[b, here, :]
        for i in range(3):
            value = value + s2b[b, i].astype(F32)
        out_ref[:, cut] = (mid[:, cut] + value).astype(out_ref.dtype)

    for cond, copies in sent:
        def run(copies=copies):
            for copy in copies:
                copy().wait_send()
        under(cond, run)


def on_device(n, tp_n, *args):
    (x_res, q_a, k_a, v_a, q_b, k_b, v_b, gain_qa, gain_ka, gain_qb, gain_kb, w_out_a, w_out_b,
     gain_mid, w_gate, w_up, conv_gate, conv_up, w_down) = args
    ff = w_gate.shape[1] // 2
    chunk, dcols = w_gate.shape[0], w_down.shape[1]
    if n != 8 or tp_n != 4 or chunk % 128 or dcols % 128 or w_gate.shape[1] % 256:
        return on_device_narrow(*args)
    rows = q_a.shape[0]
    own, width = x_res.shape
    heads_a, heads_b = q_a.shape[1] // DHA, q_b.shape[1] // DHB
    freq_a, freq_b = lane_frequencies(DHA, 2 * DHA), lane_frequencies(DHB, DHB)
    vmem = pl.BlockSpec(memory_space=pltpu.VMEM)
    hbm = pl.BlockSpec(memory_space=pltpu.MemorySpace.HBM)
    kv_width = 2 * k_a.shape[1] + 2 * k_b.shape[1]
    dma = pltpu.SemaphoreType.DMA
    scratch = [
        pltpu.VMEM((2, 4, rows, kv_width), BF16),
        pltpu.VMEM((heads_a, rows, DHA), BF16),
        pltpu.VMEM((heads_b, rows, DHB), BF16),
        pltpu.VMEM((heads_a, rows, 1), F32),
        pltpu.VMEM((heads_a, rows, 1), F32),
        pltpu.VMEM((heads_a, rows, DHA), F32),
        pltpu.VMEM((heads_b, rows, 1), F32),
        pltpu.VMEM((heads_b, rows, 1), F32),
        pltpu.VMEM((heads_b, rows, DHB), F32),
        pltpu.VMEM(w_out_a.shape, BF16),
        pltpu.VMEM(w_out_b.shape, BF16),
        pltpu.VMEM((4, 2, chunk, 2 * ff), BF16),
        pltpu.VMEM((4, chunk, 2 * ff), BF16),
        pltpu.VMEM((4, 2, ff, dcols), BF16),
        pltpu.VMEM((4, ff, dcols), BF16),
        pltpu.VMEM((rows, q_a.shape[1] + q_b.shape[1]), BF16),
        pltpu.VMEM((2, own, width), BF16),
        pltpu.VMEM((2, own, width), F32),
        pltpu.VMEM((2, own, width), BF16),
        pltpu.VMEM((own, width), BF16),
        pltpu.VMEM((own, width), BF16),
        pltpu.VMEM((own, width), F32),
        pltpu.VMEM((2, rows, width), BF16),
        pltpu.VMEM((2, rows, 2 * ff), F32),
        pltpu.VMEM((16, 2 * ff), BF16),
        pltpu.VMEM((16, 2 * ff), BF16),
        pltpu.VMEM((16, 2 * ff), BF16),
        pltpu.VMEM((2, rows, ff), BF16),
        pltpu.VMEM((n, rows, dcols), BF16),
        pltpu.VMEM((n, rows, dcols), F32),
        pltpu.VMEM((n, rows, dcols), BF16),
        pltpu.VMEM((n, 4, own, dcols), BF16),
        pltpu.VMEM((n, 3, own, dcols), BF16),
        dma((8,)),
        dma((2, 4)), dma((4,)), dma((4,)), dma((4,)),
        dma((2, 4, 2, GU_PIECES)), dma((4, 2, GU_PIECES)), dma((4, GU_PIECES)), dma((4, GU_PIECES)),
        dma((2, 4, 2, DN_PIECES)), dma((4, 2, DN_PIECES)), dma((4, DN_PIECES)), dma((4, DN_PIECES)),
        dma((2,)), dma((2,)), dma((1,)), dma((1,)),
        dma((2,)), dma((2,)), dma((1,)), dma((1,)), dma((2,)), dma((2,)), dma((4,)), dma((4,)),
        dma((2,)), dma((2,)),
        dma((n,)), dma((n,)), dma((n, 3)), dma((n, 3)),
    ]
    return pl.pallas_call(
        kernel,
        out_shape=jax.ShapeDtypeStruct(x_res.shape, BF16),
        in_specs=[vmem] * 13 + [hbm, hbm, vmem, hbm, hbm, vmem, vmem, hbm],
        out_specs=vmem,
        scratch_shapes=scratch,
        compiler_params=pltpu.CompilerParams(
            collective_id=0, has_side_effects=True, vmem_limit_bytes=60 * 1024 * 1024
        ),
        name="layer",
    )(
        x_res, q_a, jnp.transpose(k_a), jnp.transpose(v_a), q_b, k_b, v_b,
        gain_qa[None], gain_ka[None], gain_qb[None], gain_kb[None],
        freq_a, freq_b,
        w_out_a, w_out_b, gain_mid[None], w_gate, w_up, conv_gate, conv_up, w_down,
    )


def extended(block, sides, width):
    for axis, dim in sides:
        count = lax.axis_size(axis)
        forward = [(i, i + 1) for i in range(count - 1)]
        backward = [(target, source) for source, target in forward]
        low = lax.ppermute(
            lax.slice_in_dim(block, block.shape[dim] - width, None, axis=dim), axis, forward
        )
        high = lax.ppermute(lax.slice_in_dim(block, 0, width, axis=dim), axis, backward)
        block = jnp.concatenate([low, block, high], axis=dim)
    return block


def rotate_half(values):
    first, second = jnp.split(values, 2, axis=-1)
    return jnp.concatenate([-second, first], axis=-1)


def prepare(raw, gain, head_size, positions):
    count = raw.shape[0]
    heads = raw.shape[1] // head_size
    values = raw.astype(jnp.float32).reshape(count, heads, head_size)
    values = values * lax.rsqrt(jnp.mean(values * values, axis=-1, keepdims=True) + norm_eps)
    values = values * gain
    angles = rotary_angles(positions, head_size)
    cosine, sine = jnp.cos(angles), jnp.sin(angles)
    row_part, col_part = jnp.split(values, 2, axis=-1)
    turned = jnp.concatenate([rotate_half(row_part), rotate_half(col_part)], axis=-1)
    values = values * cosine[:, None, :] + turned * sine[:, None, :]
    return values.astype(jnp.bfloat16)


def start_state(queries):
    count, kv_heads, groups, head_size = queries.shape
    lowest = jnp.full((kv_heads, groups, count), -1e30, jnp.float32)
    totals = jnp.zeros((kv_heads, groups, count), jnp.float32)
    summed = jnp.zeros((kv_heads, groups, count, head_size), jnp.float32)
    return (lowest, totals, summed)


def attend(state, queries, key_piece, value_piece):
    head_size = queries.shape[3]
    kv_heads = queries.shape[1]
    length = key_piece.shape[0]
    keys = key_piece.reshape(length, kv_heads, head_size)
    values = value_piece.reshape(length, kv_heads, head_size)
    span = length
    while span > 1024 and span % 2 == 0:
        span = span // 2
    scale = jnp.float32(head_size ** (-0.5))

    def one_span(index, carry):
        running, totals, summed = carry
        key_rows = lax.dynamic_slice_in_dim(keys, index * span, span, 0)
        value_rows = lax.dynamic_slice_in_dim(values, index * span, span, 0)
        scores = (
            jnp.einsum("qkgd,skd->kgqs", queries, key_rows, preferred_element_type=jnp.float32)
            * scale
        )
        highest = jnp.maximum(running, jnp.max(scores, axis=-1))
        factor = jnp.exp(running - highest)
        expd = jnp.exp(scores - highest[..., None])
        totals = totals * factor + jnp.sum(expd, axis=-1)
        summed = summed * factor[..., None] + jnp.einsum(
            "kgqs,skd->kgqd",
            expd.astype(jnp.bfloat16),
            value_rows,
            preferred_element_type=jnp.float32,
        )
        return (highest, totals, summed)

    return lax.fori_loop(0, length // span, one_span, state)


def finish(state):
    running, totals, summed = state
    kv_heads, groups, count, head_size = summed.shape
    result = summed / totals[..., None]
    return (
        jnp.transpose(result, (2, 0, 1, 3))
        .reshape(count, kv_heads * groups * head_size)
        .astype(jnp.bfloat16)
    )


def on_device_narrow(
    x_res,
    q_a,
    k_a,
    v_a,
    q_b,
    k_b,
    v_b,
    gain_qa,
    gain_ka,
    gain_qb,
    gain_kb,
    w_out_a,
    w_out_b,
    gain_mid,
    w_gate,
    w_up,
    conv_gate,
    conv_up,
    w_down,
):
    tok_rows = q_a.shape[0]
    whole_gate, whole_up, whole_down = (
        lax.all_gather(w_gate, "sp", axis=0, tiled=True),
        lax.all_gather(w_up, "sp", axis=0, tiled=True),
        lax.all_gather(w_down, "sp", axis=1, tiled=True),
    )
    positions = lax.axis_index("sp") * tok_rows + lax.iota(jnp.int32, tok_rows)
    kv_a = k_a.shape[1] // DHA
    kv_b = k_b.shape[1] // DHB
    query_a = prepare(q_a, gain_qa, DHA, positions)
    query_a = query_a.reshape(tok_rows, kv_a, query_a.shape[1] // kv_a, DHA)
    query_b = prepare(q_b, gain_qb, DHB, positions)
    query_b = query_b.reshape(tok_rows, kv_b, query_b.shape[1] // kv_b, DHB)
    keys_a = prepare(k_a, gain_ka, DHA, positions).reshape(tok_rows, kv_a * DHA)
    keys_b = prepare(k_b, gain_kb, DHB, positions).reshape(tok_rows, kv_b * DHB)
    state_a = attend(
        start_state(query_a),
        query_a,
        lax.all_gather(keys_a, "sp", axis=0, tiled=True),
        lax.all_gather(v_a, "sp", axis=0, tiled=True),
    )
    state_b = attend(
        start_state(query_b),
        query_b,
        lax.all_gather(keys_b, "sp", axis=0, tiled=True),
        lax.all_gather(v_b, "sp", axis=0, tiled=True),
    )
    attn_a = finish(state_a)
    attn_b = finish(state_b)
    projected = lax.psum_scatter(
        (
            jnp.dot(attn_a, w_out_a, preferred_element_type=jnp.float32)
            + jnp.dot(attn_b, w_out_b, preferred_element_type=jnp.float32)
        ).astype(jnp.bfloat16),
        "tp",
        scatter_dimension=0,
        tiled=True,
    ).astype(jnp.float32)
    middle = x_res.astype(jnp.float32) + projected
    normed = middle * lax.rsqrt(jnp.mean(middle * middle, axis=-1, keepdims=True) + norm_eps)
    normed = (normed * gain_mid).astype(jnp.bfloat16)
    gathered = lax.all_gather(normed, "tp", axis=0, tiled=True)
    gate_pre = jnp.dot(gathered, whole_gate, preferred_element_type=jnp.float32)
    up_pre = jnp.dot(gathered, whole_up, preferred_element_type=jnp.float32)
    width = gate_pre.shape[1]
    joined = jnp.concatenate([gate_pre, up_pre], axis=1).astype(jnp.bfloat16)
    padded = extended(joined, (("sp", 0),), 1)
    taps = jnp.concatenate([conv_gate, conv_up], axis=1)
    mixed = padded[:-2] * taps[0] + padded[1:-1] * taps[1] + padded[2:] * taps[2]
    hidden = (jax.nn.silu(mixed[:, :width]) * mixed[:, width:]).astype(jnp.bfloat16)
    terms = jnp.dot(hidden, whole_down, preferred_element_type=jnp.float32)
    summed = lax.psum_scatter(
        terms.astype(jnp.bfloat16), "tp", scatter_dimension=0, tiled=True
    ).astype(jnp.float32)
    return (middle + summed).astype(jnp.bfloat16)


def solution(mesh):
    in_specs = (
        P(("sp", "tp"), None),
        P("sp", "tp"),
        P("sp", "tp"),
        P("sp", "tp"),
        P("sp", "tp"),
        P("sp", "tp"),
        P("sp", "tp"),
        P(),
        P(),
        P(),
        P(),
        P("tp", None),
        P("tp", None),
        P(),
        P("sp", "tp"),
        P("sp", "tp"),
        P(None, "tp"),
        P(None, "tp"),
        P("tp", "sp"),
    )
    out_specs = P(("sp", "tp"), None)
    body = functools.partial(on_device, mesh.shape["sp"], mesh.shape["tp"])
    return jax.shard_map(
        body, mesh=mesh, in_specs=in_specs, out_specs=out_specs, check_vma=False
    )
```

time: 130 us -> 105 us (0.81)
  Pallas kernels: 125 us -> 103 us
  local copies, waits for them, and re-layouts: 5.11 us -> 1.67 us
    pallas_call x1, Pallas kernels: 125 us -> 103 us  [on_device(): pl.pallas_call(kernel, out_shape=jax.ShapeDtypeStruct(x_res.shape, BF16),...]
    unnamed x5 -> x1, local copies, waits for them, and re-layouts: 3.9 us -> 1.67 us
where the time goes in v1:
time: 105 us
  Pallas kernels  103 us (98%)
  local copies, waits for them, and re-layouts  1.67 us (2%)
    pallas_call x1, Pallas kernels, on_device(): pl.pallas_call(kernel, out_shape=jax.ShapeDtypeStruct(x_res.shape, BF16),...  103 us

profile of v1, /device:TPU:0, one launch (start us, length us, event | category | flops | bytes accessed | tf_op | source)
XLA Modules:
  0.0 104.8 jit_solution(17911656777080640951)
XLA Ops:
  0.0 103.1 %layer.1 = bf16[64,2048]{1,0:T(8,128)(2,1)} custom-call(bf16[64,2048]{1,0:T(8,128)(2,1)} %x_ref.1, bf16[256,256]{1,0:T(8,128)(2,1)} %qa_ref.1, bf16[64,256]{1,0:T(8,128)(2,1)} %bitcast.7, bf16[64,256]{1,0:T(8,128)(2,1)} %bitcast.8, bf16[256,256]{1,0:T(8,128)(2,1)} %qb_ref.1, bf16[256,128]{1,0:T(8,128)(2,1)} %kb_ref.1, bf16[256,128]{1,0:T(8,128)(2,1)} %vb_ref.1, ...), custom_call_target="tpu_custom_call" | custom-call | tf_op jit(solution)/shard_map/layer/pallas_call | solution.py:696
  103.1 1.7 %copy.23 = bf16[64,2048]{1,0:T(8,128)(2,1)} copy(bf16[64,2048]{1,0:T(8,128)(2,1)} %layer.1) | data formatting | bytes 524288

commit v2 on v1

--- a/solution.py
+++ b/solution.py
@@ -18,6 +18,9 @@
 MESH = pl.DeviceIdType.MESH
 GU_PIECES = 4
 DN_PIECES = 2
+LOG2E = 1.4426950408889634
+PAIRED = True
+TAIL = 1
 
 
 def rotary_angles(positions, head_size):
@@ -72,7 +75,7 @@
     fra_ref, frb_ref,
     woa_hbm, wob_hbm, gmid_ref, wg_hbm, wu_hbm, cg_ref, cu_ref, wd_hbm,
     out_ref,
-    kv, qas, qbs, m_a, l_a, acc_a, m_b, l_b, acc_b,
+    kv, qas, qbs, m_a, acc_a, m_b, acc_b,
     woa, wob, gub, gux, dnb, dnx,
     attn, pout, own1, s1_in, q1, s2_in, mid, nrm, acc, eg_out, eg_x, eg_p, hid,
     p2, own2, s2a, q2, s2b,
@@ -167,6 +170,16 @@
                 copy().wait_recv()
         under(cond, run)
 
+    def relay(cond, arriving, *leaving):
+        def run():
+            for k, copy in enumerate(arriving):
+                copy().wait_recv()
+                for copies in leaving:
+                    copies[k]().start()
+        under(cond, run)
+        for copies in leaving:
+            sent.append((cond, copies))
+
     P = functools.partial
     gr, dr = chunk // GU_PIECES, ff // DN_PIECES
     everyp, everyd = range(GU_PIECES), range(DN_PIECES)
@@ -231,10 +244,10 @@
     for copy in loc[:4]:
         copy.wait()
     pl.semaphore_wait(barrier, 5 + u + cross)
-    go(inner, gu_to(u, h_in, 2, 0, [0]))
-    go(inner, gu_to(u, h_end, 0, 1, [0]))
+    go(inner, gu_to(u, h_in, 2, 0, [0, 1]))
+    go(inner, gu_to(u, h_end, 0, 1, [0, 1]))
     go(end, gu_to(u, h_in, 1, 0, [0]))
-    go(None, gu_over(u, [0]))
+    go(None, gu_over(u, [0, 1]))
 
     def tables(freq_ref, head):
         shape = (rows, freq_ref.shape[1])
@@ -269,9 +282,7 @@
     go(inner, [P(kv_z, u, 2, 0), P(kv_z, u, 0, 1)])
     go(end, [P(kv_z, u, 1, 0)])
     go(None, [P(kv_x, u)])
-    go(inner, gu_to(u, h_in, 2, 0, [1]) + gu_to(u, h_end, 0, 1, [1]))
     go(end, gu_to(u, h_in, 1, 0, everyp[1:]) + gu_to(u, h_end, 1, 0))
-    go(None, gu_over(u, [1]))
     for copy in loc[4:]:
         copy.wait()
     go(end, dn_to(u, h_in, 1, 0) + dn_to(u, h_end, 1, 0))
@@ -287,41 +298,55 @@
         wide(sb, heads_b * DHB), DHB,
     )
     for h in range(heads_a):
-        qas[h] = qa[:, h * DHA:(h + 1) * DHA]
+        qas[h] = jnp.concatenate([qa[:, h * DHA:(h + 1) * DHA], jnp.zeros((rows, wka), BF16)], axis=1)
     for h in range(heads_b):
         qbs[h] = qb[:, h * DHB:(h + 1) * DHB]
-    for ref, low in ((m_a, -1e30), (m_b, -1e30), (l_a, 0.0), (l_b, 0.0), (acc_a, 0.0), (acc_b, 0.0)):
+    for ref, low in ((m_a, -1e30), (m_b, -1e30), (acc_a, 0.0), (acc_b, 0.0)):
         ref[...] = jnp.full(ref.shape, low, F32)
 
-    def attend_one(queries, key_rows, value_rows, m, l, total, h):
-        scale = F32(queries.shape[2] ** (-0.5))
-        scores = lax.dot_general(
-            queries[h], key_rows, (((1,), (1,)), ((), ())), preferred_element_type=F32
-        ) * scale
+    def attend_one(query, keys, values, head, m, total, h):
+        scale = F32(head ** (-0.5) * LOG2E)
+        scores = [
+            lax.dot_general(
+                query, key, (((1,), (1,)), ((), ())), preferred_element_type=F32
+            ) * scale
+            for key in keys
+        ]
+        most = functools.reduce(jnp.maximum, scores)
         before = m[h]
-        highest = jnp.maximum(before, jnp.max(scores, axis=-1, keepdims=True))
-        factor = jnp.exp(before - highest)
-        expd = jnp.exp(scores - highest)
-        l[h] = l[h] * factor + jnp.sum(expd, axis=-1, keepdims=True)
-        total[h] = total[h] * factor + jnp.dot(
-            expd.astype(BF16), value_rows, preferred_element_type=F32
-        )
+        highest = jnp.maximum(before, jnp.max(most, axis=-1, keepdims=True))
+        factor = jnp.exp2(before - highest)
+        level = wide_to(highest, most.shape[1])
+        added = functools.reduce(jnp.add, [
+            jnp.dot(jnp.exp2(score - level).astype(BF16), value, preferred_element_type=F32)
+            for score, value in zip(scores, values)
+        ])
+        total[h] = total[h] * wide_to(factor, added.shape[1]) + added
         m[h] = highest
 
-    def attend(col, zi):
+    def wide_to(table, width):
+        return jnp.concatenate([table] * (width // table.shape[1]), axis=1)
+
+    ones_b = jnp.ones((rows, wkb), BF16)
+    is_key = lax.broadcasted_iota(jnp.int32, (rows, 2 * wka), 1) < wka
+
+    def attend(*blocks):
+        keys = [kv[col, zi, :, :wkb] for col, zi in blocks]
+        values = [
+            jnp.concatenate([kv[col, zi, :, wkb:2 * wkb], ones_b], axis=1) for col, zi in blocks
+        ]
         for h in range(heads_b):
-            attend_one(
-                qbs, kv[col, zi, :, :wkb], kv[col, zi, :, wkb:2 * wkb], m_b, l_b, acc_b, h
-            )
-        pair = kv[col, zi, :, 2 * wkb:]
+            attend_one(qbs[h], keys, values, DHB, m_b, acc_b, h)
+        keys = [kv[col, zi, :, 2 * wkb:] for col, zi in blocks]
+        values = [jnp.where(is_key, BF16(1.0), pair) for pair in keys]
         for h in range(heads_a):
-            attend_one(qas, pair[:, :wka], pair[:, wka:], m_a, l_a, acc_a, h)
+            attend_one(qas[h], keys, values, DHA, m_a, acc_a, h)
 
     def rank(k):
         high = k // 2 if isinstance(k, int) else lax.div(k, 2)
         return mz(high * k + (1 - high) * (k + u - 2 * k * u))
 
-    attend(0, z)
+    attend((0, z))
 
     def kv_crossed(zi):
         remote(
@@ -336,8 +361,7 @@
             go(None, [P(kv_x, twin)])
             got(inner, kv_in(2))
             go(inner, [P(kv_z, 2, 0, 1), P(kv_x, 2)])
-            go(inner, gu_to(u, h_in, 2, 0, everyp[2:]) + gu_to(u, h_end, 2, 0))
-            go(inner, gu_to(u, h_end, 0, 1, [2]))
+            go(inner, gu_to(u, h_in, 2, 0, everyp[2:]) + gu_to(u, h_end, 0, 1, [2]))
             go(end, gu_over(u, [2]))
 
         @pl.when(i == 2)
@@ -346,43 +370,51 @@
             go(end, [P(kv_x, 2)])
             got(inner, kv_in(3))
             go(inner, [P(kv_z, 3, 0, 1), P(kv_x, 3)])
-            go(inner, gu_to(u, h_end, 0, 1, everyp[3:]))
-            go(inner, gu_over(u, [2]))
+            go(inner, gu_to(u, h_end, 0, 1, everyp[3:]) + gu_over(u, [2]))
+            go(None, gu_over(u, everyp[3:]))
+            relay(inner, gu_in(0, h_in), gu_to(0, h_in, 2, 0), gu_over(twin))
+            go(inner, gu_to(u, h_end, 2, 0))
 
         @pl.when(i == 3)
         def _():
             got(end, kv_in(3))
             go(end, [P(kv_x, 3)])
-            go(None, gu_over(u, everyp[3:]))
-            got(inner, gu_in(2, h_end))
-            go(inner, gu_to(2, h_end, 0, 1))
-            got(inner, gu_in(0, h_in))
-            go(inner, gu_to(0, h_in, 2, 0))
-
-        attend(0, rank(i))
+            relay(inner, gu_in(2, h_end), gu_to(2, h_end, 0, 1))
+
+        if not PAIRED:
+            attend((0, rank(i)))
 
         @pl.when(i == 3)
         def _():
-            got(end, gu_in(1, my_h))
-            go(None, gu_over(twin))
-            got(inner, gu_in(0, h_end))
-            go(inner, gu_to(0, h_end, 2, 0))
-            go(inner, dn_to(u, h_in, 2, 0) + dn_to(u, h_end, 2, 0))
+            relay(end, gu_in(1, my_h), gu_over(twin))
+            relay(inner, gu_in(0, h_end), gu_to(0, h_end, 2, 0))
+            go(inner, dn_to(u, h_in, 2, 0))
 
         back = rank(i - 1)
         kv_crossed(back)
-        attend(1, back)
+        if PAIRED:
+            attend((0, rank(i)), (1, back))
+        else:
+            attend((1, back))
         return carry
 
     lax.fori_loop(1, 4, attend_step, 0)
     kv_crossed(rank(3))
-    attend(1, rank(3))
+    attend((1, rank(3)))
+
+    relay(inner, gu_in(3, h_end), gu_to(3, h_end, 0, 1))
+    got(inner, dn_in(0, h_in))
+    go(inner, dn_to(0, h_in, 2, 0) + dn_to(u, h_end, 2, 0))
+    go(None, dn_over(u))
 
     for h in range(heads_a):
-        attn[:, h * DHA:(h + 1) * DHA] = (acc_a[h] / l_a[h]).astype(BF16)
+        both = acc_a[h]
+        attn[:, h * DHA:(h + 1) * DHA] = (both[:, wka:] / both[:, :wka]).astype(BF16)
     width_a = heads_a * DHA
     for h in range(heads_b):
-        attn[:, width_a + h * DHB:width_a + (h + 1) * DHB] = (acc_b[h] / l_b[h]).astype(BF16)
+        attn[:, width_a + h * DHB:width_a + (h + 1) * DHB] = (
+            acc_b[h, :, :wkb] / acc_b[h, :, wkb:]
+        ).astype(BF16)
 
     def s1_copy(k):
         yy = (1 - y, y)[k]
@@ -410,16 +442,9 @@
     q1[...] = (own1[1 - y] + s1_in[1 - y].astype(F32)).astype(BF16)
     go(None, [s2_copy])
 
-    got(None, gu_in(2, my_h))
-    go(None, gu_over(2))
-    go(None, dn_over(u))
-    go(inner, dn_to(u, h_end, 0, 1))
-    got(inner, gu_in(3, h_end))
-    go(inner, gu_to(3, h_end, 0, 1))
-    got(inner, dn_in(0, h_in) + dn_in(0, h_end))
-    go(inner, dn_to(0, h_in, 2, 0) + dn_to(0, h_end, 2, 0))
-    got(end, dn_in(1, my_h))
-    go(None, dn_over(1 - u))
+    relay(None, gu_in(2, my_h), gu_over(2))
+    got(inner, dn_in(0, h_end))
+    go(inner, dn_to(0, h_end, 2, 0) + dn_to(u, h_end, 0, 1) + dn_over(twin))
 
     mine = pl.ds(pl.multiple_of(tp * own, own), own)
     got(None, [P(s1_copy, 1)])
@@ -457,8 +482,7 @@
 
     go(None, [P(ag_z, 0, jz), P(ag_y, tp), P(ag_z, 1, jz), P(ag_c, 0, c)])
 
-    got(None, gu_in(3, my_h))
-    go(None, gu_over(3))
+    relay(None, gu_in(3, my_h), gu_over(3))
 
     for p in range(2):
         got(None, [P(ag_z, p, 1 - jz)])
@@ -483,6 +507,9 @@
 
     acc[...] = jnp.zeros_like(acc)
     got(None, [P(ag_c, 0, 1 - c), P(ag_c, 1, 1 - c)])
+    relay(inner, dn_in(2, h_end), dn_to(2, h_end, 0, 1))
+    relay(inner, dn_in(3, h_end), dn_to(3, h_end, 0, 1))
+    relay(end, dn_in(1, my_h), dn_over(twin))
 
     def near_rows(k, carry):
         zi = rank(k)
@@ -503,6 +530,7 @@
     go(None, [P(ag_c, 3, c)])
     lax.fori_loop(2, 3, near_rows, 0)
     got(None, [P(ag_c, 2, 1 - c), P(ag_c, 3, 1 - c)])
+    relay(inner, dn_in(2, my_h), dn_over(2))
     lax.fori_loop(0, 3, other_rows, 0)
     last = mz(3)
     gate_up(jz, 0, last)
@@ -527,41 +555,46 @@
     def _():
         eg_p[...] = jnp.zeros_like(eg_p)
 
-    got(inner, dn_in(2, h_end))
-    go(inner, dn_to(2, h_end, 0, 1))
-    got(None, dn_in(2, my_h))
-    go(None, dn_over(2))
-
-    got(None, [edge_x])
-    got(cross == 1, [edge_p])
-
-    is_right = x == 1
-
-    def convolved(j, lane, taps_ref):
+    relay(end, dn_in(2, my_h), dn_over(2))
+
+    def convolved(j, lane, taps_ref, start, count, low, high):
         cut = slice(lane, lane + ff)
-        now = acc[j, :, cut].astype(BF16).astype(F32)
-        beside = eg_x[:, cut].astype(F32)
-        beyond = eg_p[:, cut].astype(F32)
-        if j == 0:
-            low = jnp.where(is_right, beside[1:2], beyond[3:4])
-            high = jnp.where(is_right, beside[2:3], beside[0:1])
-        else:
-            low = jnp.where(is_right, beside[3:4], beside[1:2])
-            high = jnp.where(is_right, beyond[0:1], beside[2:3])
+        now = acc[j, start:start + count, cut].astype(BF16).astype(F32)
         line = lax.broadcasted_iota(jnp.int32, now.shape, 0)
-        before = jnp.where(line == 0, low, pltpu.roll(now, 1, 0))
-        after = jnp.where(line == rows - 1, high, pltpu.roll(now, rows - 1, 0))
+        before = pltpu.roll(now, 1, 0)
+        after = pltpu.roll(now, count - 1, 0)
+        before = jnp.where(line == 0, 0.0 if low is None else low[:, cut], before)
+        after = jnp.where(line == count - 1, 0.0 if high is None else high[:, cut], after)
         taps = taps_ref[:, pl.ds(pl.multiple_of(my_h * ff, ff), ff)]
         return before * taps[0:1] + now * taps[1:2] + after * taps[2:3]
 
+    def gated(j, start, count, low=None, high=None):
+        gate = convolved(j, 0, cg_ref, start, count, low, high)
+        up = convolved(j, ff, cu_ref, start, count, low, high)
+        return (gate / (1.0 + jnp.exp(-gate)) * up).astype(BF16)
+
     for j in range(2):
-        gate = convolved(j, 0, cg_ref)
-        out = (gate / (1.0 + jnp.exp(-gate)) * convolved(j, ff, cu_ref)).astype(BF16)
+        out = gated(j, 0, rows)
         for yy in range(2):
             for cc in range(2):
                 at = tp_at(yy, cc) * own
                 to = (j * 2 + yy) * own
                 hid[cc, to:to + own, :] = out[at:at + own]
+
+    got(None, [edge_x])
+    got(cross == 1, [edge_p])
+
+    is_right = x == 1
+    beside, beyond = eg_x[...].astype(F32), eg_p[...].astype(F32)
+    lows = (jnp.where(is_right, beside[1:2], beyond[3:4]), jnp.where(is_right, beside[3:4], beside[1:2]))
+    highs = (jnp.where(is_right, beside[2:3], beside[0:1]), jnp.where(is_right, beyond[0:1], beside[2:3]))
+    tile, slab = 16, 32
+    for j in range(2):
+        first = gated(j, 0, slab, low=lows[j])
+        hid[0, 2 * j * own:2 * j * own + tile, :] = first[:tile]
+        final = gated(j, rows - slab, slab, high=highs[j])
+        stop = (2 * j + 2) * own
+        hid[1, stop - tile:stop, :] = final[slab - tile:]
 
     def d1_copy(b):
         return remote(p2.at[b], s2a.at[b], d1_s.at[b], d1_r.at[b], tp=tp_at(y, 1 - c))
@@ -604,16 +637,17 @@
         second_sum(0, ranks[k])
         second_sum(1, ranks[k])
 
+    def last_over(cond):
+        relay(cond, dn_in(3, my_h), dn_over(3))
+
+    last_over(inner)
     down(0)
     down(1)
     pass_on(0)
+    last_over(end)
     down(2)
     pass_on(1)
     pass_on(2)
-    got(inner, dn_in(3, h_end))
-    go(inner, dn_to(3, h_end, 0, 1))
-    got(None, dn_in(3, my_h))
-    go(None, dn_over(3))
     down(3)
     pass_on(3)
 
@@ -640,7 +674,9 @@
      gain_mid, w_gate, w_up, conv_gate, conv_up, w_down) = args
     ff = w_gate.shape[1] // 2
     chunk, dcols = w_gate.shape[0], w_down.shape[1]
-    if n != 8 or tp_n != 4 or chunk % 128 or dcols % 128 or w_gate.shape[1] % 256:
+    if n != 8 or tp_n != 4 or chunk % 128 or dcols % 128 or w_gate.shape[1] % 256 or (
+        k_a.shape[1] != DHA or k_b.shape[1] != DHB
+    ):
         return on_device_narrow(*args)
     rows = q_a.shape[0]
     own, width = x_res.shape
@@ -652,14 +688,12 @@
     dma = pltpu.SemaphoreType.DMA
     scratch = [
         pltpu.VMEM((2, 4, rows, kv_width), BF16),
-        pltpu.VMEM((heads_a, rows, DHA), BF16),
+        pltpu.VMEM((heads_a, rows, 2 * DHA), BF16),
         pltpu.VMEM((heads_b, rows, DHB), BF16),
-        pltpu.VMEM((heads_a, rows, 1), F32),
-        pltpu.VMEM((heads_a, rows, 1), F32),
-        pltpu.VMEM((heads_a, rows, DHA), F32),
-        pltpu.VMEM((heads_b, rows, 1), F32),
-        pltpu.VMEM((heads_b, rows, 1), F32),
-        pltpu.VMEM((heads_b, rows, DHB), F32),
+        pltpu.VMEM((heads_a, rows, 128), F32),
+        pltpu.VMEM((heads_a, rows, 2 * DHA), F32),
+        pltpu.VMEM((heads_b, rows, 128), F32),
+        pltpu.VMEM((heads_b, rows, 2 * DHB), F32),
         pltpu.VMEM(w_out_a.shape, BF16),
         pltpu.VMEM(w_out_b.shape, BF16),
         pltpu.VMEM((4, 2, chunk, 2 * ff), BF16),

time: 105 us -> 92.5 us (0.88)
  Pallas kernels: 103 us -> 90.7 us
    pallas_call x1, Pallas kernels: 103 us -> 90.7 us  [on_device(): pl.pallas_call(kernel, out_shape=jax.ShapeDtypeStruct(x_res.shape, BF16),...]
where the time goes in v2:
time: 92.5 us; the launch traced here: 92.4 us
  Pallas kernels  90.7 us (98%)
  local copies, waits for them, and re-layouts  1.67 us (2%)
    pallas_call x1, Pallas kernels, on_device(): pl.pallas_call(kernel, out_shape=jax.ShapeDtypeStruct(x_res.shape, BF16),...  90.7 us

profile of v2, /device:TPU:0, one launch (start us, length us, event | category | flops | bytes accessed | tf_op | source)
XLA Modules:
  0.0 92.4 jit_solution(9340770404036296396)
XLA Ops:
  0.0 90.7 %layer.1 = bf16[64,2048]{1,0:T(8,128)(2,1)} custom-call(bf16[64,2048]{1,0:T(8,128)(2,1)} %x_ref.1, bf16[256,256]{1,0:T(8,128)(2,1)} %qa_ref.1, bf16[64,256]{1,0:T(8,128)(2,1)} %bitcast.7, bf16[64,256]{1,0:T(8,128)(2,1)} %bitcast.8, bf16[256,256]{1,0:T(8,128)(2,1)} %qb_ref.1, bf16[256,128]{1,0:T(8,128)(2,1)} %kb_ref.1, bf16[256,128]{1,0:T(8,128)(2,1)} %vb_ref.1, ...), custom_call_target="tpu_custom_call" | custom-call | tf_op jit(solution)/shard_map/layer/pallas_call | solution.py:730
  90.7 1.7 %copy.23 = bf16[64,2048]{1,0:T(8,128)(2,1)} copy(bf16[64,2048]{1,0:T(8,128)(2,1)} %layer.1) | data formatting | bytes 524288

commit v3 on v2

--- a/solution.py
+++ b/solution.py
@@ -70,16 +70,18 @@
 
 
 def kernel(
+    x_in, qa_in, kat_in, vat_in, qb_in, kb_in, vb_in,
+    gqa_in, gka_in, gqb_in, gkb_in,
+    fra_in, frb_in,
+    woa_hbm, wob_hbm, gmid_in, wg_hbm, wu_hbm, cg_in, cu_in, wd_hbm,
+    out_ref,
     x_ref, qa_ref, kat_ref, vat_ref, qb_ref, kb_ref, vb_ref,
-    gqa_ref, gka_ref, gqb_ref, gkb_ref,
-    fra_ref, frb_ref,
-    woa_hbm, wob_hbm, gmid_ref, wg_hbm, wu_hbm, cg_ref, cu_ref, wd_hbm,
-    out_ref,
+    gqa_ref, gka_ref, gqb_ref, gkb_ref, fra_ref, frb_ref, gmid_ref, cg_ref, cu_ref,
     kv, qas, qbs, m_a, acc_a, m_b, acc_b,
     woa, wob, gub, gux, dnb, dnx,
     attn, pout, own1, s1_in, q1, s2_in, mid, nrm, acc, eg_out, eg_x, eg_p, hid,
     p2, own2, s2a, q2, s2b,
-    loc_sem, kvz_s, kvz_r, kvx_s, kvx_r, guz_s, guz_r, gux_s, gux_r,
+    loc_sem, in_sem, kvz_s, kvz_r, kvx_s, kvx_r, guz_s, guz_r, gux_s, gux_r,
     dnz_s, dnz_r, dnx_s, dnx_r, s1_s, s1_r, s2_s, s2_r,
     agz_s, agz_r, agy_s, agy_r, agf_s, agf_r, agc_s, agc_r, eg_s, eg_r,
     d1_s, d1_r, d2_s, d2_r,
@@ -128,6 +130,18 @@
         else:
             pl.when(cond)(signal)
 
+    staged = (
+        (kat_in, kat_ref), (vat_in, vat_ref), (kb_in, kb_ref), (vb_in, vb_ref),
+        (gka_in, gka_ref), (gkb_in, gkb_ref), (fra_in, fra_ref), (frb_in, frb_ref),
+        (qa_in, qa_ref), (qb_in, qb_ref), (gqa_in, gqa_ref), (gqb_in, gqb_ref),
+        (x_in, x_ref), (gmid_in, gmid_ref), (cg_in, cg_ref), (cu_in, cu_ref),
+    )
+    moves = [
+        pltpu.make_async_copy(src, dst, in_sem.at[k]) for k, (src, dst) in enumerate(staged)
+    ]
+    for copy in moves[:8]:
+        copy.start()
+
     loc = []
     for h in range(2):
         cut = pl.ds(h * ff, ff)
@@ -140,7 +154,7 @@
             wd_hbm.at[pl.ds(h * ff, ff)], dnb.at[z, h], loc_sem.at[len(loc)]))
     loc.append(pltpu.make_async_copy(woa_hbm, woa, loc_sem.at[len(loc)]))
     loc.append(pltpu.make_async_copy(wob_hbm, wob, loc_sem.at[len(loc)]))
-    for copy in loc:
+    for copy in loc[:4] + moves[8:12] + loc[4:] + moves[12:]:
         copy.start()
 
     def remote(src, dst, send, recv, **where):
@@ -257,6 +271,8 @@
         angles = grid.astype(F32) * freq_ref[...]
         return jnp.cos(angles), jnp.sin(angles)
 
+    for copy in moves[:8]:
+        copy.wait()
     ca, sa = tables(fra_ref, DHA)
     cb, sb = tables(frb_ref, DHB)
     wka, wkb = kat_ref.shape[0], kb_ref.shape[1]
@@ -283,7 +299,7 @@
     go(end, [P(kv_z, u, 1, 0)])
     go(None, [P(kv_x, u)])
     go(end, gu_to(u, h_in, 1, 0, everyp[1:]) + gu_to(u, h_end, 1, 0))
-    for copy in loc[4:]:
+    for copy in loc[4:] + moves[8:]:
         copy.wait()
     go(end, dn_to(u, h_in, 1, 0) + dn_to(u, h_end, 1, 0))
 
@@ -654,6 +670,12 @@
     dcols = dnx.shape[2]
     here = pl.ds(pl.multiple_of((2 * jz + y) * own, own), own)
 
+    for cond, copies in sent:
+        def run(copies=copies):
+            for copy in copies:
+                copy().wait_send()
+        under(cond, run)
+
     for b in range(own2.shape[0]):
         got(None, [P(d2_copy, b, i) for i in range(3)])
         cut = slice(b * dcols, (b + 1) * dcols)
@@ -661,12 +683,6 @@
         for i in range(3):
             value = value + s2b[b, i].astype(F32)
         out_ref[:, cut] = (mid[:, cut] + value).astype(out_ref.dtype)
-
-    for cond, copies in sent:
-        def run(copies=copies):
-            for copy in copies:
-                copy().wait_send()
-        under(cond, run)
 
 
 def on_device(n, tp_n, *args):
@@ -718,7 +734,7 @@
         pltpu.VMEM((n, rows, dcols), BF16),
         pltpu.VMEM((n, 4, own, dcols), BF16),
         pltpu.VMEM((n, 3, own, dcols), BF16),
-        dma((8,)),
+        dma((8,)), dma((16,)),
         dma((2, 4)), dma((4,)), dma((4,)), dma((4,)),
         dma((2, 4, 2, GU_PIECES)), dma((4, 2, GU_PIECES)), dma((4, GU_PIECES)), dma((4, GU_PIECES)),
         dma((2, 4, 2, DN_PIECES)), dma((4, 2, DN_PIECES)), dma((4, DN_PIECES)), dma((4, DN_PIECES)),
@@ -727,22 +743,25 @@
         dma((2,)), dma((2,)),
         dma((n,)), dma((n,)), dma((n, 3)), dma((n, 3)),
     ]
+    operands = (
+        x_res, q_a, jnp.transpose(k_a), jnp.transpose(v_a), q_b, k_b, v_b,
+        gain_qa[None], gain_ka[None], gain_qb[None], gain_kb[None],
+        freq_a, freq_b,
+        w_out_a, w_out_b, gain_mid[None], w_gate, w_up, conv_gate, conv_up, w_down,
+    )
+    small = operands[:13] + (operands[15],) + operands[18:20]
+    scratch = [pltpu.VMEM(a.shape, a.dtype) for a in small] + scratch
     return pl.pallas_call(
         kernel,
         out_shape=jax.ShapeDtypeStruct(x_res.shape, BF16),
-        in_specs=[vmem] * 13 + [hbm, hbm, vmem, hbm, hbm, vmem, vmem, hbm],
+        in_specs=[hbm] * len(operands),
         out_specs=vmem,
         scratch_shapes=scratch,
         compiler_params=pltpu.CompilerParams(
             collective_id=0, has_side_effects=True, vmem_limit_bytes=60 * 1024 * 1024
         ),
         name="layer",
-    )(
-        x_res, q_a, jnp.transpose(k_a), jnp.transpose(v_a), q_b, k_b, v_b,
-        gain_qa[None], gain_ka[None], gain_qb[None], gain_kb[None],
-        freq_a, freq_b,
-        w_out_a, w_out_b, gain_mid[None], w_gate, w_up, conv_gate, conv_up, w_down,
-    )
+    )(*operands)
 
 
 def extended(block, sides, width):

time: 92.5 us -> 91.2 us (0.986)
  Pallas kernels: 90.7 us -> 89.4 us
    pallas_call x1, Pallas kernels: 90.7 us -> 89.4 us  [on_device(): pl.pallas_call(kernel, out_shape=jax.ShapeDtypeStruct(x_res.shape, BF16),...]
where the time goes in v3:
time: 91.2 us; the launch traced here: 91.1 us
  Pallas kernels  89.4 us (98%)
  local copies, waits for them, and re-layouts  1.67 us (2%)
    pallas_call x1, Pallas kernels, on_device(): pl.pallas_call(kernel, out_shape=jax.ShapeDtypeStruct(x_res.shape, BF16),...  89.4 us

profile of v3, /device:TPU:0, one launch (start us, length us, event | category | flops | bytes accessed | tf_op | source)
XLA Modules:
  0.0 91.1 jit_solution(8020064202452104709)
XLA Ops:
  0.0 89.4 %layer.1 = bf16[64,2048]{1,0:T(8,128)(2,1)} custom-call(bf16[64,2048]{1,0:T(8,128)(2,1)} %x_in.1, bf16[256,256]{1,0:T(8,128)(2,1)} %qa_in.1, bf16[64,256]{1,0:T(8,128)(2,1)} %bitcast.7, bf16[64,256]{1,0:T(8,128)(2,1)} %bitcast.8, bf16[256,256]{1,0:T(8,128)(2,1)} %qb_in.1, bf16[256,128]{1,0:T(8,128)(2,1)} %kb_in.1, bf16[256,128]{1,0:T(8,128)(2,1)} %vb_in.1, ...), custom_call_target="tpu_custom_call" | custom-call | tf_op jit(solution)/shard_map/layer/pallas_call | solution.py:754
  89.4 1.7 %copy.23 = bf16[64,2048]{1,0:T(8,128)(2,1)} copy(bf16[64,2048]{1,0:T(8,128)(2,1)} %layer.1) | data formatting | bytes 524288
